TPU v7x, 32 devices: a whole 2x2x4 slice. The times are simulated.
32 devices in a mesh: grp: 2 (over y), sp: 8 (over z, core), tp: 2 (over x).
Axes of the slice: x: 2, y: 2, z: 4, core: 2. Of those that a mesh axis runs over, the one named last changes fastest.
Arguments:
- queries_a: bfloat16 [4096, 2, 512], P(('grp', 'sp'), None, 'tp'), parts along dimension 0, may hold values from -120 to 120
- keys_a: bfloat16 [4096, 2, 512], P(('grp', 'sp'), None, 'tp'), parts along dimension 0, may hold values from -6 to 6
- values_a: bfloat16 [4096, 1024], P(('grp', 'sp'), 'tp'), parts along dimension 0, may hold values from -6 to 6
- queries_b: bfloat16 [4096, 2, 512], P(('grp', 'sp'), None, 'tp'), parts along dimension 0, may hold values from -120 to 120
- keys_b: bfloat16 [4096, 2, 512], P(('grp', 'sp'), None, 'tp'), parts along dimension 0, may hold values from -6 to 6
- values_b: bfloat16 [4096, 1024], P(('grp', 'sp'), 'tp'), parts along dimension 0, may hold values from -6 to 6
- lambdas: float32 [12], replicated, may hold values from 0.3 to 0.8
- head_gain_a: float32 [256], replicated, may hold values from 0.1 to 1.9
- head_gain_b: float32 [128], replicated, may hold values from 0.1 to 1.9
- out_a: bfloat16 [1024, 2048], P('tp'), may hold values from -0.125 to 0.125
- out_b: bfloat16 [1024, 2048], P('tp'), may hold values from -0.125 to 0.125
- residual: bfloat16 [4096, 2048], P(('grp', 'sp', 'tp')), parts along dimension 0, may hold values from -6 to 6
- gain_mix: float32 [2048], replicated, may hold values from 0.1 to 1.9
- gain_pre: float32 [2048], replicated, may hold values from 0.1 to 1.9
- gain_post: float32 [2048], replicated, may hold values from 0.1 to 1.9
- routes: int32 [4096, 4], P(('grp', 'sp', 'tp')), parts along dimension 0, may hold values from 0 to 7, all different within a row; in each aligned block of 128 rows (0 to 127, 128 to 255, ...) at most 80 rows name the same one
- route_weights: float32 [4096, 4], P(('grp', 'sp', 'tp')), parts along dimension 0, may hold values from 0.05 to 1
- expert_gate: bfloat16 [8, 2048, 2048], P('sp', None, 'tp'), may hold values from -1 to 1
- expert_up: bfloat16 [8, 2048, 2048], P('sp', None, 'tp'), may hold values from -1 to 1
- expert_down: bfloat16 [8, 2048, 2048], P('sp', 'tp'), may hold values from -0.125 to 0.125
Outputs:
- layer_out: bfloat16 [4096, 2048], P(('grp', 'sp', 'tp')), parts along dimension 0
There are 2 independent parts, one for each index of `grp`. A program takes and returns all parts, laid end to end along the dimension named above; an argument that names none is the same for every part. Nothing has to cross between parts.
Inputs may be any that keep to these rules, and one draw needn't show every extreme that they name: `routes`: in each aligned block of 128 rows (the rows of one device) no expert is named by more than 80 rows, a bound that some blocks reach.
All inputs are finite; a program needn't handle non-finite values.
Results may differ from a plain program's by a relative error of at most 0.018.
Values may be sent and summed in bfloat16 or wider, within the bound.
A program may use at most 128 MiB of HBM per device.

v0:
```python
import jax
import jax.numpy as jnp
from jax import lax
from jax.experimental import pallas as pl
from jax.experimental.pallas import tpu as pltpu
from jax.sharding import PartitionSpec as P

HA = 4
DA = 128
DB = 64


def rms_norm(values, gain_vec):
    return values * lax.rsqrt(jnp.mean(values * values, -1, keepdims=True) + 1e-06) * gain_vec


MESH = pl.DeviceIdType.MESH
CORES = 2
PIECES = 2
LOG2E = 1.4426950408889634
VMEM_BYTES = 60 * 1024 * 1024


def place():
    sp = lax.axis_index("sp")
    return sp // CORES, sp % CORES, lax.axis_index("tp")


def greet(chips, tps):
    chip, core, tp = place()
    barrier = pltpu.get_barrier_semaphore()
    for step in range(1, chips):
        other = (chip + step) % chips
        pl.semaphore_signal(
            barrier, inc=1, device_id={"sp": other * CORES + core, "tp": tp}, device_id_type=MESH
        )
    for step in range(1, tps):
        pl.semaphore_signal(
            barrier,
            inc=1,
            device_id={"sp": chip * CORES + core, "tp": (tp + step) % tps},
            device_id_type=MESH,
        )
    pl.semaphore_signal(
        barrier, inc=1, device_id={"sp": chip * CORES + 1 - core, "tp": tp}, device_id_type=MESH
    )
    pl.semaphore_wait(barrier, chips - 1 + tps - 1 + 1)


def gather_kernel(chips, tps, own_ref, all_ref, send_sem, recv_sem, own_sem):
    chip, core, tp = place()
    greet(chips, tps)
    started = []

    def block(chip_of, core_of, tp_of, piece):
        return ((chip_of * CORES + core_of) * tps + tp_of) * PIECES + piece

    def send(source, index, sp_to, tp_to):
        copy = pltpu.make_async_remote_copy(
            src_ref=source,
            dst_ref=all_ref.at[index],
            send_sem=send_sem.at[len(started)],
            recv_sem=recv_sem.at[index],
            device_id={"sp": sp_to, "tp": tp_to},
            device_id_type=MESH,
        )
        copy.start()
        started.append(copy)

    def arrived(index):
        pltpu.make_async_copy(all_ref.at[index], all_ref.at[index], recv_sem.at[index]).wait()

    for piece in range(PIECES):
        own = block(chip, core, tp, piece)
        for step in range(1, tps):
            send(own_ref.at[piece], own, chip * CORES + core, (tp + step) % tps)
        for step in range(1, chips):
            send(own_ref.at[piece], own, (chip + step) % chips * CORES + core, tp)
        send(own_ref.at[piece], own, chip * CORES + 1 - core, tp)
    mine = pltpu.make_async_copy(
        own_ref, all_ref.at[pl.ds(block(chip, core, tp, 0), PIECES)], own_sem
    )
    mine.start()

    def from_tp(chip_of, piece):
        for step in range(1, tps):
            index = block(chip_of, core, (tp + step) % tps, piece)
            arrived(index)
            send(all_ref.at[index], index, chip * CORES + 1 - core, tp)

    order = [(step, piece) for step in range(chips) for piece in range(PIECES)]
    for place_in, (step, piece) in enumerate(order):
        if step > 0:
            index = block((chip - step + chips) % chips, core, tp, piece)
            arrived(index)
            for tp_step in range(1, tps):
                send(all_ref.at[index], index, chip * CORES + core, (tp + tp_step) % tps)
            send(all_ref.at[index], index, chip * CORES + 1 - core, tp)
            done, done_piece = order[place_in - PIECES]
            from_tp((chip - done + chips) % chips, done_piece)
    for piece in range(PIECES):
        from_tp((chip + 1) % chips, piece)
    for step, piece in order:
        for tp_of in range(tps):
            arrived(block((chip - step + chips) % chips, 1 - core, (tp + tp_of) % tps, piece))
    mine.wait()
    for copy in started:
        copy.wait_send()


def gather_rows(own, chips, tps):
    blocks = chips * CORES * tps * PIECES
    sends = (chips - 1 + tps - 1 + 1 + (chips - 1) * tps + chips * (tps - 1)) * PIECES
    rows, width = own.shape
    own = own.reshape(PIECES, rows // PIECES, width)
    return pl.pallas_call(
        lambda *refs: gather_kernel(chips, tps, *refs),
        name="gather_rows",
        out_shape=jax.ShapeDtypeStruct((blocks,) + own.shape[1:], own.dtype),
        in_specs=[pl.BlockSpec(memory_space=pl.ANY)],
        out_specs=pl.BlockSpec(memory_space=pl.ANY),
        scratch_shapes=[
            pltpu.SemaphoreType.DMA((sends,)),
            pltpu.SemaphoreType.DMA((blocks,)),
            pltpu.SemaphoreType.DMA,
        ],
        compiler_params=pltpu.CompilerParams(collective_id=1, has_side_effects=True),
    )(own).reshape(-1, rows, width)


def add_rows(target, index, source, source_index):
    rows = target.shape[1]
    chunk = min(rows, 16)

    @pl.loop(0, rows // chunk)
    def _(part):
        span = pl.ds(pl.multiple_of(part * chunk, chunk), chunk)
        target[index, span, :] = (
            target[index, span, :].astype(jnp.float32)
            + source[source_index, span, :].astype(jnp.float32)
        ).astype(target.dtype)


def scatter_kernel(
    chips, tps, part_ref, out_ref, acc, core_in, tp_in, chip_in, load_sem, send_sem, core_sem, tp_sem, chip_sem
):
    chip, core, tp = place()
    load = []
    started = []
    order = [(step, piece) for step in range(chips) for piece in range(PIECES)]
    for step, piece in order:
        for tp_step in range(tps):
            chip_of, tp_of = (chip + 1 + step) % chips, (tp + 1 + tp_step) % tps
            copy = pltpu.make_async_copy(
                part_ref.at[((chip_of * CORES + core) * tps + tp_of) * PIECES + piece],
                acc.at[(chip_of * tps + tp_of) * PIECES + piece],
                load_sem.at[len(load)],
            )
            copy.start()
            load.append(copy)
    greet(chips, tps)

    def send(source, target, recv_sem, sp_to, tp_to):
        copy = pltpu.make_async_remote_copy(
            src_ref=source,
            dst_ref=target,
            send_sem=send_sem.at[len(started)],
            recv_sem=recv_sem,
            device_id={"sp": sp_to, "tp": tp_to},
            device_id_type=MESH,
        )
        copy.start()
        started.append(copy)

    def arrived(target, index, sem):
        pltpu.make_async_copy(target.at[index], target.at[index], sem).wait()

    for step, piece in order:
        chip_of = (chip + 1 + step) % chips
        for tp_step in range(tps):
            tp_of = (tp + 1 + tp_step) % tps
            index = (chip_of * tps + tp_of) * PIECES + piece
            send(
                part_ref.at[((chip_of * CORES + 1 - core) * tps + tp_of) * PIECES + piece],
                core_in.at[index],
                core_sem.at[index],
                chip * CORES + 1 - core,
                tp,
            )

    def chip_stage(step, piece):
        chip_of = (chip + 1 + step) % chips
        kept = (chip_of * tps + tp) * PIECES + piece
        for tp_step in range(1, tps):
            index = (chip_of * tps + (tp + tp_step) % tps) * PIECES + piece
            arrived(tp_in, index, tp_sem.at[index])
            add_rows(acc, kept, tp_in, index)
        if step < chips - 1:
            slot = chip * PIECES + piece
            send(acc.at[kept], chip_in.at[slot], chip_sem.at[slot], chip_of * CORES + core, tp)

    for number, (step, piece) in enumerate(order):
        chip_of = (chip + 1 + step) % chips
        for tp_step in range(tps):
            tp_of = (tp + 1 + tp_step) % tps
            index = (chip_of * tps + tp_of) * PIECES + piece
            load[number * tps + tp_step].wait()
            arrived(core_in, index, core_sem.at[index])
            add_rows(acc, index, core_in, index)
            if tp_step < tps - 1:
                slot = (chip_of * tps + tp) * PIECES + piece
                send(
                    acc.at[index], tp_in.at[slot], tp_sem.at[slot], chip * CORES + core, tp_of
                )
        if number > 0:
            chip_stage(*order[number - 1])
    chip_stage(*order[-1])
    rows = out_ref.shape[1]
    chunk = min(rows, 16)
    for step in range(1, chips):
        for piece in range(PIECES):
            source = (chip - step + chips) % chips * PIECES + piece
            kept = (chip * tps + tp) * PIECES + piece
            arrived(chip_in, source, chip_sem.at[source])
            if step < chips - 1:
                add_rows(acc, kept, chip_in, source)
            else:

                @pl.loop(0, rows // chunk)
                def _(part):
                    span = pl.ds(pl.multiple_of(part * chunk, chunk), chunk)
                    out_ref[piece, span, :] = acc[kept, span, :].astype(jnp.float32) + chip_in[
                        source, span, :
                    ].astype(jnp.float32)

    for copy in started:
        copy.wait_send()


def scatter_rows(parts, chips, tps):
    blocks, rows, width = parts.shape
    half = chips * tps * PIECES
    sends = half + (chips * (tps - 1) + chips - 1) * PIECES
    rows = rows // PIECES
    return pl.pallas_call(
        lambda *refs: scatter_kernel(chips, tps, *refs),
        name="scatter_rows",
        out_shape=jax.ShapeDtypeStruct((PIECES, rows, width), jnp.float32),
        in_specs=[pl.BlockSpec(memory_space=pl.ANY)],
        out_specs=pl.BlockSpec(memory_space=pltpu.VMEM),
        scratch_shapes=[
            pltpu.VMEM((half, rows, width), parts.dtype),
            pltpu.VMEM((half, rows, width), parts.dtype),
            pltpu.VMEM((half, rows, width), parts.dtype),
            pltpu.VMEM((chips * PIECES, rows, width), parts.dtype),
            pltpu.SemaphoreType.DMA((half,)),
            pltpu.SemaphoreType.DMA((sends,)),
            pltpu.SemaphoreType.DMA((half,)),
            pltpu.SemaphoreType.DMA((half,)),
            pltpu.SemaphoreType.DMA((chips * PIECES,)),
        ],
        compiler_params=pltpu.CompilerParams(
            collective_id=2, has_side_effects=True, vmem_limit_bytes=VMEM_BYTES
        ),
    )(parts.reshape(-1, rows, width)).reshape(PIECES * rows, width)


def attend_kernel(
    chips, heads_a, heads_b, query_ref, own_ref, lambda_ref, gain_a_ref, gain_b_ref, out_ref,
    held, top, total, accum_a, accum_b, own_sem, up_sem, side_sem, recv_sem,
):
    chip, core, tp = place()
    me = chip * CORES + core
    rows = own_ref.shape[0]
    mine = pltpu.make_async_copy(own_ref, held.at[me], own_sem)
    mine.start()
    barrier = pltpu.get_barrier_semaphore()

    def hello(sp_to):
        pl.semaphore_signal(barrier, inc=1, device_id={"sp": sp_to, "tp": tp}, device_id_type=MESH)

    hello(chip * CORES + 1 - core)

    @pl.when(chip > 0)
    def _():
        hello(me - CORES)

    @pl.when(chip < chips - 1)
    def _():
        hello(me + CORES)

    pl.semaphore_wait(
        barrier, 1 + jnp.where(chip > 0, 1, 0) + jnp.where(chip < chips - 1, 1, 0)
    )

    top[...] = jnp.full_like(top, -1e30)
    total[...] = jnp.zeros_like(total)
    accum_a[...] = jnp.zeros_like(accum_a)
    accum_b[...] = jnp.zeros_like(accum_b)
    mine.wait()

    def copy_up(back, index):
        return pltpu.make_async_remote_copy(
            src_ref=held.at[index], dst_ref=held.at[index], send_sem=up_sem.at[back],
            recv_sem=recv_sem.at[index], device_id={"sp": me + CORES, "tp": tp}, device_id_type=MESH,
        )

    def copy_side(back, index):
        return pltpu.make_async_remote_copy(
            src_ref=held.at[index], dst_ref=held.at[index], send_sem=side_sem.at[back],
            recv_sem=recv_sem.at[index], device_id={"sp": chip * CORES + 1 - core, "tp": tp},
            device_id_type=MESH,
        )

    base_va = 2 * heads_a * DA
    base_kb = base_va + heads_a * 2 * DA
    base_vb = base_kb + 2 * heads_b * DB
    base_qb = 2 * heads_a * DA
    ahead = lax.broadcasted_iota(jnp.int32, (rows, rows), 0) - lax.broadcasted_iota(
        jnp.int32, (rows, rows), 1
    )

    def flash(index):
        shown = ahead + (me - index) * rows >= 0

        def one(slot, query, key, value, accum, part, size):
            scores = lax.dot_general(
                query, key, (((1,), (1,)), ((), ())), preferred_element_type=jnp.float32
            )
            scores = jnp.where(shown, scores, -1e30)
            before = top[slot]
            after = jnp.maximum(before, jnp.max(scores, -1, keepdims=True))
            factor = size ** (-0.5) * LOG2E
            terms = jnp.exp2((scores - after) * factor)
            rescale = jnp.exp2((before - after) * factor)
            top[slot] = after
            total[slot] = total[slot] * rescale + jnp.sum(terms, -1, keepdims=True)
            accum[part] = accum[part] * rescale + jnp.dot(
                terms.astype(jnp.bfloat16), value, preferred_element_type=jnp.float32
            )

        for head in range(heads_a):
            value = held[index, :, base_va + head * 2 * DA : base_va + (head + 1) * 2 * DA]
            for pair in range(2):
                at = (pair * heads_a + head) * DA
                part = pair * heads_a + head
                one(
                    part, query_ref[:, at : at + DA], held[index, :, at : at + DA], value,
                    accum_a, part, DA,
                )
        for head in range(heads_b):
            value = held[index, :, base_vb + head * 2 * DB : base_vb + (head + 1) * 2 * DB]
            for pair in range(2):
                part = pair * heads_b + head
                at = base_qb + part * 2 * DB
                key_at = base_kb + part // 2 * 2 * DB
                one(
                    2 * heads_a + part, query_ref[:, at : at + 2 * DB],
                    held[index, :, key_at : key_at + 2 * DB], value, accum_b, part, DB,
                )

    def step(number, carry):
        back = number // 2
        side = number % 2
        source = chip - back

        @pl.when(source >= 0)
        def _():
            index = source * CORES + jnp.where(side == 0, core, 1 - core)

            @pl.when(number > 0)
            def _():
                pltpu.make_async_copy(held.at[index], held.at[index], recv_sem.at[index]).wait()

            @pl.when(side == 0)
            def _():
                @pl.when(chip < chips - 1)
                def _():
                    copy_up(back, index).start()

                copy_side(back, index).start()

            @pl.when(index <= me)
            def _():
                flash(index)

        return carry

    lax.fori_loop(0, 2 * chips, step, 0)

    def finish(head, parts, accum, slots, lam, gain_ref, at, wide):
        mixture = accum[parts[0]] / total[slots[0]] - lam * accum[parts[1]] / total[slots[1]]
        out_ref[:, at : at + wide] = rms_norm(mixture, gain_ref[...]).astype(out_ref.dtype)

    for head in range(heads_a):
        parts = (head, heads_a + head)
        finish(head, parts, accum_a, parts, lambda_ref[0:1, head : head + 1], gain_a_ref,
               head * 2 * DA, 2 * DA)
    for head in range(heads_b):
        parts = (head, heads_b + head)
        slots = (2 * heads_a + head, 2 * heads_a + heads_b + head)
        finish(head, parts, accum_b, slots, lambda_ref[0:1, heads_a + head : heads_a + head + 1],
               gain_b_ref, heads_a * 2 * DA + head * 2 * DB, 2 * DB)

    def settle(back, carry):
        @pl.when(chip - back >= 0)
        def _():
            index = (chip - back) * CORES + core

            @pl.when(chip < chips - 1)
            def _():
                copy_up(back, index).wait_send()

            copy_side(back, index).wait_send()

        return carry

    lax.fori_loop(0, chips, settle, 0)


def attend_blocks(queries, own, lambdas, gain_a, gain_b, chips, heads_a, heads_b):
    rows, width = own.shape
    vmem = pl.BlockSpec(memory_space=pltpu.VMEM)
    return pl.pallas_call(
        lambda *refs: attend_kernel(chips, heads_a, heads_b, *refs),
        name="attend_blocks",
        out_shape=jax.ShapeDtypeStruct((rows, heads_a * 2 * DA + heads_b * 2 * DB), jnp.bfloat16),
        in_specs=[vmem, pl.BlockSpec(memory_space=pl.ANY), vmem, vmem, vmem],
        out_specs=vmem,
        scratch_shapes=[
            pltpu.VMEM((chips * CORES, rows, width), own.dtype),
            pltpu.VMEM((2 * (heads_a + heads_b), rows, 1), jnp.float32),
            pltpu.VMEM((2 * (heads_a + heads_b), rows, 1), jnp.float32),
            pltpu.VMEM((2 * heads_a, rows, 2 * DA), jnp.float32),
            pltpu.VMEM((2 * heads_b, rows, 2 * DB), jnp.float32),
            pltpu.SemaphoreType.DMA,
            pltpu.SemaphoreType.DMA((chips,)),
            pltpu.SemaphoreType.DMA((chips,)),
            pltpu.SemaphoreType.DMA((chips * CORES,)),
        ],
        compiler_params=pltpu.CompilerParams(
            collective_id=3, has_side_effects=True, vmem_limit_bytes=VMEM_BYTES
        ),
    )(queries, own, lambdas, gain_a, gain_b)


def share_kernel(tps, part_ref, out_ref, arrived, send_sem, recv_sem):
    tp = lax.axis_index("tp")
    barrier = pltpu.get_barrier_semaphore()
    for step in range(1, tps):
        pl.semaphore_signal(barrier, inc=1, device_id={"tp": (tp + step) % tps}, device_id_type=MESH)
    pl.semaphore_wait(barrier, tps - 1)
    started = []
    for step in range(1, tps):
        other = (tp + step) % tps
        copy = pltpu.make_async_remote_copy(
            src_ref=part_ref.at[other], dst_ref=arrived.at[step - 1], send_sem=send_sem.at[step - 1],
            recv_sem=recv_sem.at[step - 1], device_id={"tp": other}, device_id_type=MESH,
        )
        copy.start()
        started.append(copy)
    rows = out_ref.shape[0]
    chunk = min(rows, 16)
    for step in range(1, tps):
        started[step - 1].wait()

        @pl.loop(0, rows // chunk)
        def _(part):
            span = pl.ds(pl.multiple_of(part * chunk, chunk), chunk)
            first = part_ref[tp, span, :].astype(jnp.float32) if step == 1 else out_ref[span, :]
            out_ref[span, :] = first + arrived[step - 1, span, :].astype(jnp.float32)


def share_rows(parts, tps):
    _, rows, width = parts.shape
    vmem = pl.BlockSpec(memory_space=pltpu.VMEM)
    return pl.pallas_call(
        lambda *refs: share_kernel(tps, *refs),
        name="share_rows",
        out_shape=jax.ShapeDtypeStruct((rows, width), jnp.float32),
        in_specs=[vmem],
        out_specs=vmem,
        scratch_shapes=[
            pltpu.VMEM((tps - 1, rows, width), parts.dtype),
            pltpu.SemaphoreType.DMA((tps - 1,)),
            pltpu.SemaphoreType.DMA((tps - 1,)),
        ],
        compiler_params=pltpu.CompilerParams(collective_id=4, has_side_effects=True),
    )(parts)


def spread_pairs(queries, heads):
    rows = queries.shape[0]
    pairs = queries.reshape(rows, 2 * heads // 2, 1, 2, DB)
    keep = jnp.eye(2, dtype=queries.dtype).reshape(1, 1, 2, 2, 1)
    return (pairs * keep).reshape(rows, 2 * heads * 2 * DB)


def expert_parts(gathered, expert, experts, capacity, width, weights):
    gate, up, down = weights
    blocks, rows, _ = gathered.shape
    shares = lax.dynamic_slice_in_dim(gathered[:, :, width:], expert, 1, 2)[:, :, 0]
    named = shares > 0
    order = jnp.arange(rows, dtype=jnp.int32)
    slots = jnp.dot(
        named.astype(jnp.bfloat16),
        (order[:, None] < order[None, :]).astype(jnp.bfloat16),
        preferred_element_type=jnp.float32,
    ).astype(jnp.int32)
    picks = (slots[:, None, :] == jnp.arange(capacity, dtype=jnp.int32)[None, :, None]) & named[:, None, :]
    rows_in = jnp.einsum(
        "bct,btd->bcd",
        picks.astype(jnp.bfloat16),
        gathered[:, :, :width],
        preferred_element_type=jnp.float32,
    ).astype(jnp.bfloat16)
    rows_in = rows_in.reshape(blocks * capacity, width)
    gate_pre = jnp.dot(rows_in, gate, preferred_element_type=jnp.float32)
    up_pre = jnp.dot(rows_in, up, preferred_element_type=jnp.float32)
    glu_part = jnp.minimum(gate_pre, 7.0)
    lin_part = jnp.clip(up_pre, -7.0, 7.0)
    hidden = (glu_part * jax.nn.sigmoid(1.702 * glu_part) * (lin_part + 1.0)).astype(jnp.bfloat16)
    outs = jnp.dot(hidden, down, preferred_element_type=jnp.float32).astype(jnp.bfloat16)
    back = jnp.where(picks, shares[:, None, :], 0).astype(jnp.bfloat16)
    return jnp.einsum(
        "bct,bcd->btd",
        back,
        outs.reshape(blocks, capacity, width),
        preferred_element_type=jnp.float32,
    ).astype(jnp.bfloat16)


def per_device(
    queries_a,
    keys_a,
    values_a,
    queries_b,
    keys_b,
    values_b,
    lambdas,
    head_gain_a,
    head_gain_b,
    out_a,
    out_b,
    residual,
    gain_mix,
    gain_pre,
    gain_post,
    routes,
    route_weights,
    expert_gate,
    expert_up,
    expert_down,
):
    length = queries_a.shape[0]
    heads_a = queries_a.shape[2] // DA
    heads_b = queries_b.shape[2] // DB
    head_slot = lax.axis_index("tp")
    seq_slot = lax.axis_index("sp")
    lambda_a = lax.dynamic_slice_in_dim(lambdas, head_slot * heads_a, heads_a)
    lambda_b = lax.dynamic_slice_in_dim(lambdas, HA + head_slot * heads_b, heads_b)
    experts, tps = lax.axis_size("sp"), lax.axis_size("tp")
    chips = experts // CORES
    own = jnp.concatenate(
        [keys_a.reshape(length, -1), values_a, keys_b.reshape(length, -1), values_b], 1
    )
    queries = jnp.concatenate([queries_a.reshape(length, -1), spread_pairs(queries_b, heads_b)], 1)
    heads_out = attend_blocks(
        queries,
        own,
        jnp.concatenate([lambda_a, lambda_b])[None],
        head_gain_a[None],
        head_gain_b[None],
        chips,
        heads_a,
        heads_b,
    )
    cut = heads_a * 2 * DA
    mixed = (
        jnp.dot(heads_out[:, :cut], out_a, preferred_element_type=jnp.float32)
        + jnp.dot(heads_out[:, cut:], out_b, preferred_element_type=jnp.float32)
    ).astype(jnp.bfloat16)
    mixed_rows = share_rows(mixed.reshape(tps, length // tps, -1), tps)
    after_mix = (residual.astype(jnp.float32) + rms_norm(mixed_rows, gain_mix)).astype(jnp.bfloat16)
    normed = rms_norm(after_mix.astype(jnp.float32), gain_pre).astype(jnp.bfloat16)
    sub_rows = residual.shape[0]
    top_count = routes.shape[1]
    capacity = min(sub_rows, (5 * sub_rows * top_count + 4 * experts - 1) // (4 * experts))
    width = residual.shape[1]
    extra = -(-experts // 128) * 128
    shares = jnp.sum(
        jnp.where(
            routes[:, :, None] == jnp.arange(extra, dtype=jnp.int32)[None, None, :],
            route_weights[:, :, None],
            0.0,
        ),
        1,
    ).astype(jnp.bfloat16)
    gathered = gather_rows(jnp.concatenate([normed, shares], 1), chips, tps)
    parts = expert_parts(
        gathered, seq_slot, experts, capacity, width, (expert_gate[0], expert_up[0], expert_down[0])
    )
    routed = scatter_rows(parts, chips, tps)
    return (after_mix.astype(jnp.float32) + rms_norm(routed, gain_post)).astype(jnp.bfloat16)


def solution(mesh):
    in_specs = (
        P(("grp", "sp"), None, "tp"),
        P(("grp", "sp"), None, "tp"),
        P(("grp", "sp"), "tp"),
        P(("grp", "sp"), None, "tp"),
        P(("grp", "sp"), None, "tp"),
        P(("grp", "sp"), "tp"),
        P(),
        P(),
        P(),
        P("tp", None),
        P("tp", None),
        P(("grp", "sp", "tp"), None),
        P(),
        P(),
        P(),
        P(("grp", "sp", "tp"), None),
        P(("grp", "sp", "tp"), None),
        P("sp", None, "tp"),
        P("sp", None, "tp"),
        P("sp", "tp", None),
    )
    out_specs = P(("grp", "sp", "tp"), None)
    return jax.shard_map(
        per_device, mesh=mesh, in_specs=in_specs, out_specs=out_specs, check_vma=False
    )
```

profile of v0, /device:TPU:0, one launch (start us, length us, event | category | flops | bytes accessed | tf_op | source)
XLA Modules:
  0.0 300.4 jit_solution(15533948815563409269)
XLA Ops:
  0.0 0.0 copy-start
  0.0 0.9 dynamic_slice.10
  0.9 0.7 dynamic_slice.9
  1.6 0.6 maximum_bitcast_fusion.refs_2_
  2.2 0.1 mul.101
  2.3 0.1 mul.102
  2.4 0.9 select_reduce_fusion
  3.3 1.0 copy.29
  4.2 1.7 copy.30
  5.9 1.1 copy.27
  7.1 0.2 copy.28
  7.4 0.9 pad_maximum_fusion.1.refs_0_
  8.3 1.0 copy.31
  9.3 2.2 pad_maximum_fusion.refs_1_
  11.5 27.9 %attend_blocks.1 = bf16[256,1024]{1,0:T(8,128)(2,1)} custom-call(bf16[256,1536]{1,0:T(8,128)(2,1)} %pad_maximum_fusion.1.refs_0_, bf16[256,2048]{1,0:T(8,128)(2,1)} %pad_maximum_fusion.refs_1_, f32[1,6]{1,0:T(1,128)} %maximum_bitcast_fusion.refs_2_, f32[1,256]{1,0:T(1,128)} %bitcast.57, f32[1,128]{1,0:T(1,128)} %bitcast.58), custom_call_target="tpu_custom_call" | custom-call | tf_op jit(solution)/shard_map/attend_blocks/pallas_call | solution.py:424
  39.4 0.0 copy-done
  39.4 0.0 copy-start.2
  39.5 1.8 fusion.30
  41.3 0.0 copy-done.2
  41.3 0.0 copy-start.3
  41.3 0.0 copy-start.4
  41.3 0.0 copy-start.5
  41.3 2.7 fusion.15
  44.1 15.2 %share_rows.1 = f32[128,2048]{1,0:T(8,128)} custom-call(bf16[2,128,2048]{2,1,0:T(8,128)(2,1)} %bitcast.47), custom_call_target="tpu_custom_call" | custom-call | tf_op jit(solution)/shard_map/share_rows/pallas_call | solution.py:477
  59.2 1.4 multiply_reduce_fusion.1
  60.6 0.0 copy-done.3
  60.6 0.0 copy-done.4
  60.6 1.6 fusion.16
  62.2 0.0 copy-done.5
  62.2 0.2 fusion.18
  62.4 0.9 pad_maximum_fusion.2
  63.3 120.6 %gather_rows.1 = bf16[32,64,2176]{2,1,0:T(8,128)(2,1)} custom-call(bf16[2,64,2176]{2,1,0:T(8,128)(2,1)} %bitcast.48), custom_call_target="tpu_custom_call" | custom-call | tf_op jit(solution)/shard_map/gather_rows/pallas_call | solution.py:116
  183.9 1.1 slice.16
  185.0 0.4 dynamic-slice_reduce_fusion
  185.4 0.1 convolution_convert_fusion.2
  185.5 0.0 copy-start.7
  185.5 5.1 %fusion.6 = bf16[16,80,2048]{2,1,0:T(8,128)(2,1)S(1)} fusion(bf16[16,128,2176]{2,1,0:T(8,128)(2,1)} %bitcast.42, s32[16,128]{1,0:T(8,128)S(1)} %convolution_convert_fusion.2, pred[16,128]{1,0:T(8,128)(4,1)S(1)} %broadcast_compare_fusion), kind=kOutput, calls=%fused_computation.9 | convolution fusion | flops 674037760 | bytes 13641728 | tf_op jit(solution)/shard_map/bct,btd->bcd/dot_general | solution.py:511
  190.6 0.0 copy-start.1
  190.6 2.4 copy-done.1
  193.0 0.0 copy-done.7
  193.0 7.3 %fusion.4 = f32[1280,1024]{1,0:T(8,128)} fusion(bf16[1280,2048]{1,0:T(8,128)(2,1)S(1)} %bitcast.44, bf16[1,2048,1024]{2,1,0:T(8,128)(2,1)S(1)} %copy-done.7), kind=kOutput, calls=%fused_computation.7 | convolution fusion | flops 5368709120 | bytes 14680064 | tf_op jit(solution)/shard_map/dot_general | solution.py:518
  200.3 18.7 %convolution_convert_fusion = bf16[1280,2048]{1,0:T(8,128)(2,1)} fusion(bf16[1,1024,2048]{2,1,0:T(8,128)(2,1)} %param.39, f32[1280,1024]{1,0:T(8,128)} %fusion.4, bf16[1280,2048]{1,0:T(8,128)(2,1)} %bitcast.45, bf16[1,2048,1024]{2,1,0:T(8,128)(2,1)} %param.38), kind=kOutput, calls=%fused_computation.2 | convolution fusion | flops 10753146880 | bytes 24117248 | tf_op jit(solution)/shard_map/dot_general | solution.py:523
  219.0 8.2 %convolution_convert_fusion.1 = bf16[16,128,2048]{2,1,0:T(8,128)(2,1)} fusion(bf16[16,80,2048]{2,1,0:T(8,128)(2,1)} %bitcast.46, s32[16,128]{1,0:T(8,128)S(1)} %convolution_convert_fusion.2, pred[16,128]{1,0:T(8,128)(4,1)S(1)} %broadcast_compare_fusion, bf16[16,128]{1,0:T(8,128)(2,1)S(1)} %dynamic-slice_reduce_fusion), kind=kOutput, calls=%fused_computation.3 | convolution fusion | flops 675774464 | bytes 13645824 | tf_op jit(solution)/shard_map/bct,bcd->btd/dot_general | solution.py:525
  227.2 69.5 %scatter_rows.1 = f32[2,64,2048]{2,1,0:T(8,128)} custom-call(bf16[32,64,2048]{2,1,0:T(8,128)(2,1)} %bitcast.43), custom_call_target="tpu_custom_call" | custom-call | tf_op jit(solution)/shard_map/scatter_rows/pallas_call | solution.py:245
  296.7 1.4 multiply_reduce_fusion
  298.0 0.1 rsqrt.30
  298.1 0.0 copy-done.6
  298.1 2.3 fusion.19
  (8 shorter events, 0.1 us)
Async XLA Ops:
  0.0 39.4 %copy-start = (bf16[512,2048]{1,0:T(8,128)(2,1)S(1)}, bf16[512,2048]{1,0:T(8,128)(2,1)}, u32[]{:S(2)}) copy-start(bf16[512,2048]{1,0:T(8,128)(2,1)} %param.29) | copy-start | bytes 6291460
  39.4 1.8 copy-start.2
  41.3 19.3 %copy-start.3 = (bf16[128,2048]{1,0:T(8,128)(2,1)S(1)}, bf16[128,2048]{1,0:T(8,128)(2,1)}, u32[]{:S(2)}) copy-start(bf16[128,2048]{1,0:T(8,128)(2,1)} %param.31) | copy-start | bytes 1572868
  41.3 19.3 %copy-start.4 = (f32[2048]{0:T(1024)S(1)}, f32[2048]{0:T(1024)}, u32[]{:S(2)}) copy-start(f32[2048]{0:T(1024)} %param.32) | copy-start | bytes 24580
  41.3 20.9 %copy-start.5 = (f32[2048]{0:T(1024)S(1)}, f32[2048]{0:T(1024)}, u32[]{:S(2)}) copy-start(f32[2048]{0:T(1024)} %param.33) | copy-start | bytes 24580
  185.5 7.4 %copy-start.7 = (bf16[1,2048,1024]{2,1,0:T(8,128)(2,1)S(1)}, bf16[1,2048,1024]{2,1,0:T(8,128)(2,1)}, u32[]{:S(2)}) copy-start(bf16[1,2048,1024]{2,1,0:T(8,128)(2,1)} %param.37) | copy-start | bytes 12582916
  190.6 2.4 copy-start.1
  227.2 70.9 %copy-start.6 = (f32[2048]{0:T(1024)S(1)}, f32[2048]{0:T(1024)}, u32[]{:S(2)}) copy-start(f32[2048]{0:T(1024)} %param.34) | copy-start | bytes 24580
where the time goes:
time: 301 us; the launch traced here: 300 us
  Pallas kernels  233 us (77%)
  matrix products  44 us (15%)
  other arithmetic  12.4 us (4%)
  local copies, waits for them, and re-layouts  10.7 us (4%)
    pallas_call x1, Pallas kernels, gather_rows(): pl.pallas_call(lambda *refs: gather_kernel(chips, tps, *refs), name='gath...  121 us
    pallas_call x1, Pallas kernels, scatter_rows(): pl.pallas_call(lambda *refs: scatter_kernel(chips, tps, *refs), name='sca...  69.5 us
    pallas_call x1, Pallas kernels, attend_blocks(): pl.pallas_call(lambda *refs: attend_kernel(chips, heads_a, heads_b, *refs...  27.9 us
    dot_general x1, matrix products, expert_parts(): jnp.dot(hidden, down, preferred_element_type=jnp.float32)  18.7 us
    pallas_call x1, Pallas kernels, share_rows(): pl.pallas_call(lambda *refs: share_kernel(tps, *refs), name='share_rows',...  15.2 us
    dot_general x1, matrix products, expert_parts(): jnp.einsum('bct,bcd->btd', back, outs.reshape(blocks, capacity, width), p...  8.19 us
    dot_general x1, matrix products, expert_parts(): gate_pre = jnp.dot(rows_in, gate, preferred_element_type=jnp.float32)  7.35 us
    unnamed x20, local copies, waits for them, and re-layouts  7.15 us

commit v1 on v0

--- a/solution.py
+++ b/solution.py
@@ -528,6 +528,440 @@
         outs.reshape(blocks, capacity, width),
         preferred_element_type=jnp.float32,
     ).astype(jnp.bfloat16)
+
+
+def meet(chips, tps):
+    chip, core, tp = place()
+    barrier = pltpu.get_barrier_semaphore()
+    others = 0
+    for chip_step in range(chips):
+        for core_step in range(CORES):
+            for tp_step in range(tps):
+                if chip_step + core_step + tp_step > 0:
+                    others += 1
+                    pl.semaphore_signal(
+                        barrier,
+                        inc=1,
+                        device_id={
+                            "sp": (chip + chip_step) % chips * CORES + (core + core_step) % CORES,
+                            "tp": (tp + tp_step) % tps,
+                        },
+                        device_id_type=MESH,
+                    )
+    pl.semaphore_wait(barrier, others)
+
+
+def group_at(chip, chips, step):
+    near = jnp.minimum(chip, chips - 1 - chip)
+    both = jnp.where(step % 2 == 1, chip - (step + 1) // 2, chip + step // 2)
+    past = jnp.where(chip <= chips - 1 - chip, chip + step - near, chip - step + near)
+    return jnp.where(step <= 2 * near, both, past)
+
+
+def experts_kernel(
+    chips, tps, capacity,
+    own_ref, meta_ref, gate_ref, up_ref, down_ref, out_ref,
+    rows_all, meta_all, gate, up, down, rows_in, hidden, back, part, core_in, x_in, z_in,
+    load_sem, weight_sem, row_sem, meta_send, meta_recv, up_sem, dn_sem, x_sem, side_sem,
+    core_send, core_recv, xs_send, xs_recv, zs_send, zs_recv,
+):
+    chip, core, tp = place()
+    experts = meta_ref.shape[0] // 2
+    piece_rows, width = rows_all.shape[2], rows_all.shape[3]
+    rows = piece_rows * PIECES
+    ff = gate.shape[1]
+    members = CORES * tps
+    side_sp = chip * CORES + 1 - core
+
+    def blk(chip_of, core_of, tp_of):
+        return (chip_of * CORES + core_of) * tps + tp_of
+
+    def remote(src, dst, send, recv, sp_to, tp_to):
+        return pltpu.make_async_remote_copy(
+            src_ref=src, dst_ref=dst, send_sem=send, recv_sem=recv,
+            device_id={"sp": sp_to, "tp": tp_to}, device_id_type=MESH,
+        )
+
+    def rows_copy(block, piece, send, sp_to, tp_to):
+        ref = rows_all.at[block, piece]
+        return remote(ref, ref, send, row_sem.at[block, piece], sp_to, tp_to)
+
+    def go_up(chip_of, piece):
+        return rows_copy(blk(chip_of, core, tp), piece, up_sem.at[chip_of, piece],
+                         (chip + 1) * CORES + core, tp)
+
+    def go_dn(chip_of, piece):
+        return rows_copy(blk(chip_of, core, tp), piece, dn_sem.at[chip_of, piece],
+                         (chip - 1) * CORES + core, tp)
+
+    def go_x(chip_of, step, piece):
+        return rows_copy(blk(chip_of, core, tp), piece, x_sem.at[chip_of, step - 1, piece],
+                         chip * CORES + core, (tp + step) % tps)
+
+    def go_side(chip_of, tp_of, piece):
+        return rows_copy(blk(chip_of, core, tp_of), piece, side_sem.at[chip_of, tp_of, piece],
+                         side_sp, tp)
+
+    def wait_rows(block, piece):
+        ref = rows_all.at[block, piece]
+        pltpu.make_async_copy(ref, ref, row_sem.at[block, piece]).wait()
+
+    mine = blk(chip, core, tp)
+    loads = [
+        pltpu.make_async_copy(own_ref.at[piece], rows_all.at[mine, piece], load_sem.at[piece])
+        for piece in range(PIECES)
+    ]
+    weights = [
+        pltpu.make_async_copy(src, dst, weight_sem.at[number])
+        for number, (src, dst) in enumerate(((gate_ref, gate), (up_ref, up), (down_ref, down)))
+    ]
+    for copy in loads + weights:
+        copy.start()
+    meta_all[mine] = meta_ref[...]
+    meet(chips, tps)
+
+    for piece in range(PIECES):
+        loads[piece].wait()
+        for step in range(1, tps):
+            go_x(chip, step, piece).start()
+
+        @pl.when(chip < chips - 1)
+        def _():
+            go_up(chip, piece).start()
+
+        @pl.when(chip > 0)
+        def _():
+            go_dn(chip, piece).start()
+
+        go_side(chip, tp, piece).start()
+
+    def meta_copy(number, chip_step, core_step, tp_step):
+        return remote(
+            meta_ref, meta_all.at[mine], meta_send.at[number], meta_recv.at[mine],
+            (chip + chip_step) % chips * CORES + (core + core_step) % CORES, (tp + tp_step) % tps,
+        )
+
+    meta_steps = [
+        (chip_step, core_step, tp_step)
+        for chip_step in range(chips) for core_step in range(CORES) for tp_step in range(tps)
+        if chip_step + core_step + tp_step > 0
+    ]
+    for number, steps in enumerate(meta_steps):
+        meta_copy(number, *steps).start()
+
+    def relay(chip_of, piece, upward):
+        wait_rows(blk(chip_of, core, tp), piece)
+        for step in range(1, tps):
+            go_x(chip_of, step, piece).start()
+        if upward:
+            @pl.when(chip < chips - 1)
+            def _():
+                go_up(chip_of, piece).start()
+        else:
+            @pl.when(chip > 0)
+            def _():
+                go_dn(chip_of, piece).start()
+        go_side(chip_of, tp, piece).start()
+
+    def compute(group):
+        order = lax.broadcasted_iota(jnp.int32, (capacity, rows), 0).astype(jnp.float32)
+        expert = chip * CORES + core
+        for member in range(members):
+            block = group * members + member
+            slot = meta_all[block, pl.ds(expert, 1), :]
+            share = meta_all[block, pl.ds(experts + expert, 1), :]
+            hit = slot == order
+            picks = jnp.where(hit, 1.0, 0.0).astype(jnp.bfloat16)
+            back[member] = jnp.where(hit, share, 0.0).astype(jnp.bfloat16)
+            values = rows_all[block].reshape(rows, width)
+            rows_in[member * capacity : (member + 1) * capacity, :] = jnp.dot(
+                picks, values, preferred_element_type=jnp.float32
+            ).astype(jnp.bfloat16)
+        cut = min(ff, 256)
+
+        @pl.loop(0, ff // cut)
+        def _(number):
+            cols = pl.ds(pl.multiple_of(number * cut, cut), cut)
+            gate_pre = jnp.dot(rows_in[...], gate[:, cols], preferred_element_type=jnp.float32)
+            up_pre = jnp.dot(rows_in[...], up[:, cols], preferred_element_type=jnp.float32)
+            glu_part = jnp.minimum(gate_pre, 7.0)
+            lin_part = jnp.clip(up_pre, -7.0, 7.0)
+            hidden[:, cols] = (
+                glu_part * jax.nn.sigmoid(1.702 * glu_part) * (lin_part + 1.0)
+            ).astype(jnp.bfloat16)
+
+        wide = min(width, 256)
+
+        @pl.loop(0, width // wide)
+        def _(number):
+            cols = pl.ds(pl.multiple_of(number * wide, wide), wide)
+            outs = jnp.dot(
+                hidden[...], down[:, cols], preferred_element_type=jnp.float32
+            ).astype(jnp.bfloat16)
+            for member in range(members):
+                spread = lax.dot_general(
+                    back[member], outs[member * capacity : (member + 1) * capacity],
+                    (((0,), (0,)), ((), ())), preferred_element_type=jnp.float32,
+                ).astype(jnp.bfloat16)
+                part[group * members + member, :, :, cols] = spread.reshape(
+                    PIECES, piece_rows, wide
+                )
+
+    def add(target, index, source, source_index):
+        chunk = min(piece_rows, 16)
+
+        @pl.loop(0, piece_rows // chunk)
+        def _(number):
+            span = pl.ds(pl.multiple_of(number * chunk, chunk), chunk)
+            target[index + (span,)] = (
+                target[index + (span,)].astype(jnp.float32)
+                + source[source_index + (span,)].astype(jnp.float32)
+            ).astype(target.dtype)
+
+    def core_copy(group, tp_of):
+        return remote(part.at[blk(group, 1 - core, tp_of)], core_in.at[group, tp_of],
+                      core_send.at[group, tp_of], core_recv.at[group, tp_of], side_sp, tp)
+
+    def part_x(group, step, piece):
+        return remote(part.at[blk(group, core, (tp + step) % tps), piece],
+                      x_in.at[group, step - 1, piece], xs_send.at[group, step - 1, piece],
+                      xs_recv.at[group, step - 1, piece], chip * CORES + core, (tp + step) % tps)
+
+    def part_z(way, group, piece):
+        return remote(part.at[blk(group, core, tp), piece], z_in.at[way, group, piece],
+                      zs_send.at[way, group, piece], zs_recv.at[way, group, piece],
+                      (chip + 1 - 2 * way) * CORES + core, tp)
+
+    def arrived(ref, sem):
+        pltpu.make_async_copy(ref, ref, sem).wait()
+
+    def cross(group):
+        for tp_of in range(tps):
+            core_copy(group, tp_of).start()
+        for step in list(range(1, tps)) + [0]:
+            tp_of = (tp + step) % tps
+            arrived(core_in.at[group, tp_of], core_recv.at[group, tp_of])
+            for piece in range(PIECES):
+                add(part, (blk(group, core, tp_of), piece), core_in, (group, tp_of, piece))
+                if step > 0:
+                    part_x(group, step, piece).start()
+
+    def settle(group):
+        for piece in range(PIECES):
+            for step in range(1, tps):
+                arrived(x_in.at[group, step - 1, piece], xs_recv.at[group, step - 1, piece])
+                add(part, (blk(group, core, tp), piece), x_in, (group, step - 1, piece))
+
+            @pl.when((chip == 0) & (group > 0))
+            def _():
+                part_z(0, group, piece).start()
+
+            @pl.when((chip == chips - 1) & (group < chips - 1))
+            def _():
+                part_z(1, group, piece).start()
+
+    def wave(step, carry):
+        @pl.when(step < chips)
+        def _():
+            for piece in range(PIECES):
+                @pl.when(chip - step >= 0)
+                def _():
+                    relay(chip - step, piece, True)
+
+                @pl.when(chip + step < chips)
+                def _():
+                    relay(chip + step, piece, False)
+
+        group = group_at(chip, chips, step - 1)
+        for piece in range(PIECES):
+            for tp_step in range(1, tps):
+                tp_of = (tp + tp_step) % tps
+                wait_rows(blk(group, core, tp_of), piece)
+                go_side(group, tp_of, piece).start()
+
+        @pl.when(step == 1)
+        def _():
+            for steps in meta_steps:
+                block = blk((chip + steps[0]) % chips, (core + steps[1]) % CORES, (tp + steps[2]) % tps)
+                arrived(meta_all.at[block], meta_recv.at[block])
+            for copy in weights:
+                copy.wait()
+
+        for piece in range(PIECES):
+            for tp_of in range(tps):
+                wait_rows(blk(group, 1 - core, tp_of), piece)
+        compute(group)
+        cross(group)
+
+        @pl.when(step > 1)
+        def _():
+            settle(group_at(chip, chips, step - 2))
+
+        return carry
+
+    lax.fori_loop(1, chips + 1, wave, 0)
+    settle(group_at(chip, chips, chips - 1))
+
+    def chain(number, carry):
+        for way in range(2):
+            group = number if way == 0 else chips - 1 - number
+            if way == 0:
+                passes = (chip > 0) & (chip < group)
+            else:
+                passes = (chip < chips - 1) & (chip > group)
+
+            @pl.when(passes)
+            def _():
+                for piece in range(PIECES):
+                    arrived(z_in.at[way, group, piece], zs_recv.at[way, group, piece])
+                    add(part, (blk(group, core, tp), piece), z_in, (way, group, piece))
+                    part_z(way, group, piece).start()
+
+        return carry
+
+    lax.fori_loop(1, chips, chain, 0)
+
+    chunk = min(piece_rows, 16)
+    for piece in range(PIECES):
+        @pl.loop(0, piece_rows // chunk)
+        def _(number):
+            span = pl.ds(pl.multiple_of(number * chunk, chunk), chunk)
+            out_ref[piece, span, :] = part[mine, piece, span, :].astype(jnp.float32)
+
+        for way in range(2):
+            @pl.when(chip > 0 if way == 0 else chip < chips - 1)
+            def _():
+                arrived(z_in.at[way, chip, piece], zs_recv.at[way, chip, piece])
+
+                @pl.loop(0, piece_rows // chunk)
+                def _(number):
+                    span = pl.ds(pl.multiple_of(number * chunk, chunk), chunk)
+                    out_ref[piece, span, :] = out_ref[piece, span, :] + z_in[
+                        way, chip, piece, span, :
+                    ].astype(jnp.float32)
+
+    for number, steps in enumerate(meta_steps):
+        meta_copy(number, *steps).wait_send()
+
+    def finish(group, carry):
+        for piece in range(PIECES):
+            for step in range(1, tps):
+                go_x(group, step, piece).wait_send()
+                part_x(group, step, piece).wait_send()
+            for tp_of in range(tps):
+                go_side(group, tp_of, piece).wait_send()
+
+            @pl.when((group <= chip) & (chip < chips - 1))
+            def _():
+                go_up(group, piece).wait_send()
+
+            @pl.when((group >= chip) & (chip > 0))
+            def _():
+                go_dn(group, piece).wait_send()
+
+            @pl.when(group > chip)
+            def _():
+                part_z(0, group, piece).wait_send()
+
+            @pl.when(group < chip)
+            def _():
+                part_z(1, group, piece).wait_send()
+
+        for tp_of in range(tps):
+            core_copy(group, tp_of).wait_send()
+        return carry
+
+    lax.fori_loop(0, chips, finish, 0)
+
+
+def experts_bytes(rows, width, ff, chips, tps, capacity):
+    blocks = chips * CORES * tps
+    members = CORES * tps
+    buffers = blocks * 2 + chips * (2 * tps - 1 + 2) + 2
+    return 2 * (
+        rows * width * buffers + 3 * width * ff + members * capacity * (width + ff) + 2 * rows * width
+    )
+
+
+def run_experts(normed, meta, gate, up, down, chips, tps, capacity):
+    rows, width = normed.shape
+    ff = gate.shape[1]
+    blocks = chips * CORES * tps
+    members = CORES * tps
+    piece_rows = rows // PIECES
+    vmem = pl.BlockSpec(memory_space=pltpu.VMEM)
+    any_space = pl.BlockSpec(memory_space=pl.ANY)
+    dma = pltpu.SemaphoreType.DMA
+    bf16 = jnp.bfloat16
+    return pl.pallas_call(
+        lambda *refs: experts_kernel(chips, tps, capacity, *refs),
+        name="run_experts",
+        out_shape=jax.ShapeDtypeStruct((PIECES, piece_rows, width), jnp.float32),
+        in_specs=[any_space, vmem, any_space, any_space, any_space],
+        out_specs=vmem,
+        scratch_shapes=[
+            pltpu.VMEM((blocks, PIECES, piece_rows, width), bf16),
+            pltpu.VMEM((blocks,) + meta.shape, meta.dtype),
+            pltpu.VMEM(gate.shape, bf16),
+            pltpu.VMEM(up.shape, bf16),
+            pltpu.VMEM(down.shape, bf16),
+            pltpu.VMEM((members * capacity, width), bf16),
+            pltpu.VMEM((members * capacity, ff), bf16),
+            pltpu.VMEM((members, capacity, rows), bf16),
+            pltpu.VMEM((blocks, PIECES, piece_rows, width), bf16),
+            pltpu.VMEM((chips, tps, PIECES, piece_rows, width), bf16),
+            pltpu.VMEM((chips, tps - 1, PIECES, piece_rows, width), bf16),
+            pltpu.VMEM((2, chips, PIECES, piece_rows, width), bf16),
+            dma((PIECES,)),
+            dma((3,)),
+            dma((blocks, PIECES)),
+            dma((blocks - 1,)),
+            dma((blocks,)),
+            dma((chips, PIECES)),
+            dma((chips, PIECES)),
+            dma((chips, tps - 1, PIECES)),
+            dma((chips, tps, PIECES)),
+            dma((chips, tps)),
+            dma((chips, tps)),
+            dma((chips, tps - 1, PIECES)),
+            dma((chips, tps - 1, PIECES)),
+            dma((2, chips, PIECES)),
+            dma((2, chips, PIECES)),
+        ],
+        compiler_params=pltpu.CompilerParams(
+            collective_id=5, has_side_effects=True, vmem_limit_bytes=VMEM_BYTES
+        ),
+    )(normed.reshape(PIECES, piece_rows, width), meta, gate, up, down).reshape(rows, width)
+
+
+def slot_table(routes, route_weights, experts):
+    rows = routes.shape[0]
+    chosen = routes[None, :, :] == jnp.arange(experts, dtype=jnp.int32)[:, None, None]
+    shares = jnp.sum(jnp.where(chosen, route_weights[None], 0.0), 2)
+    named = jnp.any(chosen, 2)
+    order = jnp.arange(rows, dtype=jnp.int32)
+    slots = jnp.dot(
+        named.astype(jnp.bfloat16),
+        (order[:, None] < order[None, :]).astype(jnp.bfloat16),
+        preferred_element_type=jnp.float32,
+    )
+    return jnp.concatenate([jnp.where(named, slots, -1.0), shares], 0)
+
+
+def spread_experts(normed, routes, route_weights, seq_slot, experts, capacity, chips, tps, weights):
+    width = normed.shape[1]
+    extra = -(-experts // 128) * 128
+    shares = jnp.sum(
+        jnp.where(
+            routes[:, :, None] == jnp.arange(extra, dtype=jnp.int32)[None, None, :],
+            route_weights[:, :, None],
+            0.0,
+        ),
+        1,
+    ).astype(jnp.bfloat16)
+    gathered = gather_rows(jnp.concatenate([normed, shares], 1), chips, tps)
+    parts = expert_parts(gathered, seq_slot, experts, capacity, width, weights)
+    return scatter_rows(parts, chips, tps)
 
 
 def per_device(
@@ -587,20 +1021,17 @@
     top_count = routes.shape[1]
     capacity = min(sub_rows, (5 * sub_rows * top_count + 4 * experts - 1) // (4 * experts))
     width = residual.shape[1]
-    extra = -(-experts // 128) * 128
-    shares = jnp.sum(
-        jnp.where(
-            routes[:, :, None] == jnp.arange(extra, dtype=jnp.int32)[None, None, :],
-            route_weights[:, :, None],
-            0.0,
-        ),
-        1,
-    ).astype(jnp.bfloat16)
-    gathered = gather_rows(jnp.concatenate([normed, shares], 1), chips, tps)
-    parts = expert_parts(
-        gathered, seq_slot, experts, capacity, width, (expert_gate[0], expert_up[0], expert_down[0])
-    )
-    routed = scatter_rows(parts, chips, tps)
+    slots = -(-capacity // 16) * 16
+    if experts_bytes(sub_rows, width, expert_gate.shape[2], chips, tps, slots) < VMEM_BYTES * 9 // 10:
+        routed = run_experts(
+            normed, slot_table(routes, route_weights, experts), expert_gate[0], expert_up[0],
+            expert_down[0], chips, tps, slots,
+        )
+    else:
+        routed = spread_experts(
+            normed, routes, route_weights, seq_slot, experts, capacity, chips, tps,
+            (expert_gate[0], expert_up[0], expert_down[0]),
+        )
     return (after_mix.astype(jnp.float32) + rms_norm(routed, gain_post)).astype(jnp.bfloat16)
 
 

time: 301 us -> 262 us (0.87)
  matrix products: 44 us -> 3.66 us
  Pallas kernels: 233 us -> 243 us
  local copies, waits for them, and re-layouts: 10.7 us -> 3.37 us
    dot_general x5 -> x1, matrix products: 39.4 us -> 0.13 us  [slot_table(): jnp.dot(named.astype(jnp.bfloat16), (order[:, None] < order[None, :]).ast...]
    pallas_call x2 -> x1, Pallas kernels: 190 us -> 200 us  [run_experts(): pl.pallas_call(lambda *refs: experts_kernel(chips, tps, capacity, *refs),...]
    unnamed x20 -> x32, local copies, waits for them, and re-layouts: 7.15 us -> 1.26 us
where the time goes in v1:
time: 262 us
  Pallas kernels  243 us (93%)
  other arithmetic  11 us (4%)
  matrix products  3.66 us (1%)
  local copies, waits for them, and re-layouts  3.37 us (1%)
    pallas_call x1, Pallas kernels, run_experts(): pl.pallas_call(lambda *refs: experts_kernel(chips, tps, capacity, *refs),...  200 us
    pallas_call x1, Pallas kernels, attend_blocks(): pl.pallas_call(lambda *refs: attend_kernel(chips, heads_a, heads_b, *refs...  28 us
    pallas_call x1, Pallas kernels, share_rows(): pl.pallas_call(lambda *refs: share_kernel(tps, *refs), name='share_rows',...  15.3 us

profile of v1, /device:TPU:0, one launch (start us, length us, event | category | flops | bytes accessed | tf_op | source)
XLA Modules:
  0.0 261.6 jit_solution(13255659755760932301)
XLA Ops:
  0.0 0.0 copy-start
  0.0 0.0 copy-start.4
  0.0 0.9 dynamic_slice.6
  0.9 0.7 dynamic_slice.7
  1.6 0.6 maximum_bitcast_fusion.refs_2_
  2.2 1.1 copy.27
  3.4 0.2 copy.28
  3.6 0.0 copy-start.5
  3.6 0.0 copy-start.6
  3.6 0.1 mul.89
  3.7 0.1 mul.90
  3.8 0.0 copy-start.7
  3.8 0.0 copy-start.8
  3.8 0.0 copy-done.4
  3.9 1.0 pad_maximum_fusion.1.refs_0_
  4.8 0.0 copy-done.5
  4.9 0.0 copy-done.6
  4.9 0.0 copy-done.7
  4.9 0.0 copy-done.8
  5.0 1.1 pad_maximum_fusion.refs_1_
  6.1 28.0 %attend_blocks.1 = bf16[256,1024]{1,0:T(8,128)(2,1)} custom-call(bf16[256,1536]{1,0:T(8,128)(2,1)} %pad_maximum_fusion.1.refs_0_, bf16[256,2048]{1,0:T(8,128)(2,1)} %pad_maximum_fusion.refs_1_, f32[1,6]{1,0:T(1,128)} %maximum_bitcast_fusion.refs_2_, f32[1,256]{1,0:T(1,128)} %bitcast.39, f32[1,128]{1,0:T(1,128)} %bitcast.40), custom_call_target="tpu_custom_call" | custom-call | tf_op jit(solution)/shard_map/attend_blocks/pallas_call | solution.py:424
  34.1 0.0 copy-done
  34.1 0.0 copy-start.1
  34.1 0.0 copy-start.2
  34.1 1.8 fusion.7
  35.9 0.0 copy-done.1
  35.9 0.0 copy-done.2
  35.9 1.7 fusion
  37.6 0.0 copy-start.3
  37.6 15.3 %share_rows.1 = f32[128,2048]{1,0:T(8,128)} custom-call(bf16[2,128,2048]{2,1,0:T(8,128)(2,1)} %bitcast.29), custom_call_target="tpu_custom_call" | custom-call | tf_op jit(solution)/shard_map/share_rows/pallas_call | solution.py:477
  52.9 0.0 copy-start.10
  52.9 0.0 copy-start.12
  52.9 0.0 copy-start.13
  53.0 1.4 multiply_reduce_fusion.1
  54.4 0.0 copy-done.3
  54.4 0.0 copy-done.9
  54.4 1.6 fusion.1
  56.0 0.0 copy-done.10
  56.0 1.0 fusion.3
  57.0 0.0 copy-done.12
  57.0 0.1 convolution_select_fusion
  57.1 0.0 copy-done.13
  57.1 0.6 pad_maximum_fusion.2.refs_1_
  57.7 200.1 %run_experts.1 = f32[2,64,2048]{2,1,0:T(8,128)} custom-call(bf16[2,64,2048]{2,1,0:T(8,128)(2,1)} %bitcast.30, f32[16,128]{1,0:T(8,128)} %pad_maximum_fusion.2.refs_1_, bf16[2048,1024]{1,0:T(8,128)(2,1)} %bitcast.26, bf16[2048,1024]{1,0:T(8,128)(2,1)} %bitcast.27, bf16[1024,2048]{1,0:T(8,128)(2,1)} %bitcast.28), custom_call_target="tpu_custom_call" | custom-call | tf_op jit(solution)/shard_map/run_experts/pallas_call | solution.py:896
  257.9 1.4 multiply_reduce_fusion
  259.3 0.1 rsqrt.30
  259.3 0.0 copy-done.11
  259.4 2.3 fusion.4
  (13 shorter events, 0.2 us)
Async XLA Ops:
  0.0 34.1 %copy-start = (bf16[512,2048]{1,0:T(8,128)(2,1)S(1)}, bf16[512,2048]{1,0:T(8,128)(2,1)}, u32[]{:S(2)}) copy-start(bf16[512,2048]{1,0:T(8,128)(2,1)} %param.29) | copy-start | bytes 6291460
  0.0 3.8 %copy-start.4 = (bf16[256,2,256]{2,1,0:T(2,128)(2,1)S(1)}, bf16[256,2,256]{2,1,0:T(2,128)(2,1)}, u32[]{:S(2)}) copy-start(bf16[256,2,256]{2,1,0:T(2,128)(2,1)} %param.20) | copy-start | bytes 786436
  3.6 1.3 copy-start.5
  3.6 1.3 copy-start.6
  3.8 1.2 copy-start.7
  3.8 1.2 copy-start.8
  34.1 1.8 copy-start.1
  34.1 1.8 copy-start.2
  37.6 16.7 %copy-start.3 = (bf16[128,2048]{1,0:T(8,128)(2,1)S(1)}, bf16[128,2048]{1,0:T(8,128)(2,1)}, u32[]{:S(2)}) copy-start(bf16[128,2048]{1,0:T(8,128)(2,1)} %param.31) | copy-start | bytes 1572868
  37.6 16.7 %copy-start.9 = (f32[2048]{0:T(1024)S(1)}, f32[2048]{0:T(1024)}, u32[]{:S(2)}) copy-start(f32[2048]{0:T(1024)} %param.32) | copy-start | bytes 24580
  52.9 3.1 %copy-start.10 = (f32[2048]{0:T(1024)S(1)}, f32[2048]{0:T(1024)}, u32[]{:S(2)}) copy-start(f32[2048]{0:T(1024)} %param.33) | copy-start | bytes 24580
  52.9 4.0 %copy-start.12 = (s32[128,4]{0,1:T(4,128)S(1)}, s32[128,4]{0,1:T(4,128)}, u32[]{:S(2)}) copy-start(s32[128,4]{0,1:T(4,128)} %param.35) | copy-start | bytes 6148
  52.9 4.2 %copy-start.13 = (f32[128,4]{0,1:T(4,128)S(1)}, f32[128,4]{0,1:T(4,128)}, u32[]{:S(2)}) copy-start(f32[128,4]{0,1:T(4,128)} %param.36) | copy-start | bytes 6148
  57.7 201.6 %copy-start.11 = (f32[2048]{0:T(1024)S(1)}, f32[2048]{0:T(1024)}, u32[]{:S(2)}) copy-start(f32[2048]{0:T(1024)} %param.34) | copy-start | bytes 24580

commit v2 on v1

--- a/solution.py
+++ b/solution.py
@@ -17,6 +17,7 @@
 MESH = pl.DeviceIdType.MESH
 CORES = 2
 PIECES = 2
+CUTS = 4
 LOG2E = 1.4426950408889634
 VMEM_BYTES = 60 * 1024 * 1024
 
@@ -440,6 +441,366 @@
         ],
         compiler_params=pltpu.CompilerParams(
             collective_id=3, has_side_effects=True, vmem_limit_bytes=VMEM_BYTES
+        ),
+    )(queries, own, lambdas, gain_a, gain_b)
+
+
+def pivots_of(chips, slices):
+    return [1, chips - 2, 0, chips - 2] if slices == chips == 4 else None
+
+
+def sliced_kernel(
+    chips, tps, heads_a, heads_b, pivots,
+    q_ref, own_ref, lambda_ref, gain_a_ref, gain_b_ref, out_ref,
+    kvs, qs, accum, top, total, o_out, o_all,
+    load_sem, q_send, q_recv, dn_send, up_send, kv_recv, side_send, o_send, o_recv,
+):
+    chip, core, tp = place()
+    rows = out_ref.shape[0]
+    slices = len(pivots)
+    key_width = 2 * DA
+    me = chip * CORES + core
+
+    def pivot(number):
+        if isinstance(number, int):
+            return pivots[number]
+        return sum(jnp.where(number == n, pivots[n], 0) for n in range(slices))
+
+    loads = []
+    for number in range(slices):
+        if number < heads_a:
+            head, stride, q_at, k_at = number, heads_a * DA, 0, 0
+        else:
+            head, stride = number - heads_a, heads_b * DB
+            q_at, k_at = 2 * heads_a * DA, 4 * heads_a * DA
+        v_at = k_at + 2 * stride + head * 2 * DA
+        moves = []
+        for pair in range(2):
+            at = pair * stride + head * DA
+            spot = pl.ds(pair * DA, DA)
+            moves.append((q_ref.at[:, pl.ds(q_at + at, DA)], qs.at[chip, number, :, spot]))
+            moves.append((own_ref.at[:, pl.ds(k_at + at, DA)], kvs.at[me, number, :, spot]))
+        moves.append(
+            (own_ref.at[:, pl.ds(v_at, 2 * DA)], kvs.at[me, number, :, pl.ds(key_width, 2 * DA)])
+        )
+        loads.append([
+            pltpu.make_async_copy(src, dst, load_sem.at[number, place_in])
+            for place_in, (src, dst) in enumerate(moves)
+        ])
+    order = sorted(range(slices), key=lambda n: pivots[n])
+    for number in order:
+        for copy in loads[number]:
+            copy.start()
+    greet(chips, 1)
+
+    def remote(src, dst, send, recv, sp_to):
+        return pltpu.make_async_remote_copy(
+            src_ref=src, dst_ref=dst, send_sem=send, recv_sem=recv,
+            device_id={"sp": sp_to, "tp": tp}, device_id_type=MESH,
+        )
+
+    def send_q(number):
+        ref = qs.at[chip, number]
+        return remote(ref, ref, q_send.at[number], q_recv.at[chip, number],
+                      pivot(number) * CORES + core)
+
+    def send_kv(number, chip_to, sem):
+        ref = kvs.at[me, number]
+        return remote(ref, ref, sem, kv_recv.at[me, number], chip_to * CORES + core)
+
+    def send_dn(number):
+        return send_kv(number, pivot(number), dn_send.at[number])
+
+    def send_up(number, step):
+        return send_kv(number, chip + step, up_send.at[number, step - 1])
+
+    def send_side(chip_of, number):
+        ref = kvs.at[chip_of * CORES + core, number]
+        return remote(ref, ref, side_send.at[chip_of, number],
+                      kv_recv.at[chip_of * CORES + core, number], chip * CORES + 1 - core)
+
+    def send_out(query, number):
+        return remote(o_out.at[query, number], o_all.at[number], o_send.at[query, number],
+                      o_recv.at[number], query * CORES + core)
+
+    def arrived(ref, sem):
+        pltpu.make_async_copy(ref, ref, sem).wait()
+
+    for number in order:
+        for copy in loads[number]:
+            copy.wait()
+
+        @pl.when(chip > pivots[number])
+        def _():
+            send_q(number).start()
+
+        @pl.when(chip <= pivots[number])
+        def _():
+            send_side(chip, number).start()
+
+    for number in order:
+        @pl.when(chip > pivots[number])
+        def _():
+            send_dn(number).start()
+
+    for step in reversed(range(1, chips)):
+        for number in order:
+            @pl.when(chip + step <= pivots[number])
+            def _():
+                send_up(number, step).start()
+
+    ahead = lax.broadcasted_iota(jnp.int32, (rows, rows), 0) - lax.broadcasted_iota(
+        jnp.int32, (rows, rows), 1
+    )
+    low_half = lax.broadcasted_iota(jnp.int32, (rows, DA), 1) < DB
+
+    def step_one(query, number, slot, q, kv_chip, pair, v_at, wide, acc_at, size, masked):
+        tiles = []
+        for side in range(CORES):
+            key = kvs[kv_chip * CORES + side, number, :, pair * DA : (pair + 1) * DA]
+            scores = lax.dot_general(
+                q, key, (((1,), (1,)), ((), ())), preferred_element_type=jnp.float32
+            )
+            if masked:
+                scores = jnp.where(ahead + (core - side) * rows >= 0, scores, -1e30)
+            tiles.append(scores)
+        before = top[query, number, slot]
+        after = jnp.maximum(
+            before, jnp.max(jnp.maximum(tiles[0], tiles[1]), -1, keepdims=True)
+        )
+        factor = size ** (-0.5) * LOG2E
+        terms = [jnp.exp2((scores - after) * factor) for scores in tiles]
+        rescale = jnp.exp2((before - after) * factor)
+        top[query, number, slot] = after
+        total[query, number, slot] = total[query, number, slot] * rescale + jnp.sum(
+            terms[0] + terms[1], -1, keepdims=True
+        )
+        fresh = sum(
+            jnp.dot(
+                terms[side].astype(jnp.bfloat16),
+                kvs[kv_chip * CORES + side, number, :, v_at : v_at + wide],
+                preferred_element_type=jnp.float32,
+            )
+            for side in range(CORES)
+        )
+        span = slice(acc_at, acc_at + wide)
+        accum[query, number, pair, :, span] = accum[query, number, pair, :, span] * rescale + fresh
+
+    def flash_a(query, kv_chip, number, masked):
+        for pair in range(2):
+            step_one(query, number, pair, qs[query, number, :, pair * DA : (pair + 1) * DA],
+                     kv_chip, pair, key_width, 2 * DA, 0, DA, masked)
+
+    def flash_b(query, kv_chip, number, masked):
+        for pair in range(2):
+            both = qs[query, number, :, pair * DA : (pair + 1) * DA]
+            for head in range(2):
+                keep = low_half if head == 0 else jnp.logical_not(low_half)
+                q = jnp.where(keep, both, jnp.zeros_like(both))
+                step_one(query, number, pair * 2 + head, q, kv_chip, pair,
+                         key_width + head * 2 * DB, 2 * DB, head * 2 * DB, DB, masked)
+
+    def relevant(query, number):
+        return jnp.where(query == chip, pivot(number) >= chip, pivot(number) == chip)
+
+    def over(body):
+        def run_a(number, carry):
+            body(number, flash_a)
+            return carry
+
+        def run_b(number, carry):
+            body(number, flash_b)
+            return carry
+
+        lax.fori_loop(0, heads_a, run_a, 0)
+        lax.fori_loop(heads_a, slices, run_b, 0)
+
+    def pair_up(query, kv_chip, first):
+        def body(number, flash):
+            @pl.when(relevant(query, number))
+            def _():
+                @pl.when(first)
+                def _():
+                    top[query, number] = jnp.full(top.shape[2:], -1e30, jnp.float32)
+                    total[query, number] = jnp.zeros(total.shape[2:], jnp.float32)
+                    accum[query, number] = jnp.zeros(accum.shape[2:], jnp.float32)
+
+                @pl.when(query == kv_chip)
+                def _():
+                    flash(query, kv_chip, number, True)
+
+                @pl.when(query != kv_chip)
+                def _():
+                    flash(query, kv_chip, number, False)
+
+        over(body)
+
+    def mix(query, number, slots, spans, lam, gain_ref):
+        mixture = (
+            accum[query, number, 0, :, spans] / total[query, number, slots[0]]
+            - lam * accum[query, number, 1, :, spans] / total[query, number, slots[1]]
+        )
+        return rms_norm(mixture, gain_ref[...]).astype(jnp.bfloat16)
+
+    def finish(query):
+        def body(number, flash):
+            @pl.when(relevant(query, number))
+            def _():
+                if flash is flash_a:
+                    lam = lambda_ref[0, tp * heads_a + number]
+                    made = [mix(query, number, (0, 1), slice(0, 2 * DA), lam, gain_a_ref)]
+                else:
+                    made = []
+                    for head in range(2):
+                        lam = lambda_ref[
+                            0, tps * heads_a + tp * heads_b + (number - heads_a) * 2 + head
+                        ]
+                        made.append(
+                            mix(query, number, (head, 2 + head),
+                                slice(head * 2 * DB, (head + 1) * 2 * DB), lam, gain_b_ref)
+                        )
+                wide = 2 * DA // len(made)
+                for place_in, values in enumerate(made):
+                    span = slice(place_in * wide, (place_in + 1) * wide)
+
+                    @pl.when(query == chip)
+                    def _():
+                        o_all[number, :, span] = values
+
+                    @pl.when(query != chip)
+                    def _():
+                        o_out[query, number, :, span] = values
+
+                @pl.when(query != chip)
+                def _():
+                    send_out(query, number).start()
+
+        over(body)
+
+    above = chips - 1 - chip
+
+    def event(number_of, carry):
+        is_own = number_of == 0
+        is_query = (number_of > 0) & (number_of <= above)
+        is_below = (number_of > above) & (number_of <= above + chip)
+        is_above = number_of > above + chip
+        source = jnp.where(
+            number_of <= above,
+            chip + number_of,
+            jnp.where(is_below, chip - (number_of - above), number_of - above),
+        )
+        kv_chip = jnp.where(number_of <= above, chip, source)
+        low = jnp.where(is_below, chip, source)
+        high = jnp.where(number_of <= above, source, chips - 1)
+
+        def wait_q(number, carry):
+            @pl.when(is_query & (pivot(number) == chip))
+            def _():
+                arrived(qs.at[source, number], q_recv.at[source, number])
+
+            return carry
+
+        def needs(number):
+            return jnp.where(source > chip, pivot(number) == chip, pivot(number) >= chip)
+
+        def wait_kv(number, carry):
+            @pl.when((is_below | is_above) & needs(number))
+            def _():
+                index = source * CORES + core
+                arrived(kvs.at[index, number], kv_recv.at[index, number])
+                send_side(source, number).start()
+
+            return carry
+
+        def wait_side(number, carry):
+            @pl.when((is_own | is_below | is_above) & needs(number))
+            def _():
+                index = source * CORES + 1 - core
+                arrived(kvs.at[index, number], kv_recv.at[index, number])
+
+            return carry
+
+        lax.fori_loop(0, slices, wait_q, 0)
+        lax.fori_loop(0, slices, wait_kv, 0)
+        lax.fori_loop(0, slices, wait_side, 0)
+
+        def queries(query, carry):
+            pair_up(query, kv_chip, kv_chip == chip)
+
+            @pl.when(
+                ((query == chip) & (number_of == jnp.where(chip > 0, above + chip, 0)))
+                | (is_above & (query == source))
+            )
+            def _():
+                finish(query)
+
+            return carry
+
+        lax.fori_loop(low, high + 1, queries, 0)
+        return carry
+
+    lax.fori_loop(0, 1 + above + chips - 1, event, 0)
+
+    for number in range(slices):
+        @pl.when(chip > pivots[number])
+        def _():
+            arrived(o_all.at[number], o_recv.at[number])
+
+        out_ref[:, number * 2 * DA : (number + 1) * 2 * DA] = o_all[number]
+
+    for number in range(slices):
+        @pl.when(chip > pivots[number])
+        def _():
+            send_q(number).wait_send()
+            send_dn(number).wait_send()
+
+        for step in range(1, chips):
+            @pl.when(chip + step <= pivots[number])
+            def _():
+                send_up(number, step).wait_send()
+
+        for chip_of in range(chips):
+            @pl.when(jnp.where(chip_of > chip, pivots[number] == chip, pivots[number] >= chip))
+            def _():
+                send_side(chip_of, number).wait_send()
+
+            @pl.when((chip_of > chip) & (pivots[number] == chip))
+            def _():
+                send_out(chip_of, number).wait_send()
+
+
+def attend_sliced(queries, own, lambdas, gain_a, gain_b, chips, tps, heads_a, heads_b, pivots):
+    rows = own.shape[0]
+    slices = len(pivots)
+    vmem = pl.BlockSpec(memory_space=pltpu.VMEM)
+    any_space = pl.BlockSpec(memory_space=pl.ANY)
+    dma = pltpu.SemaphoreType.DMA
+    return pl.pallas_call(
+        lambda *refs: sliced_kernel(chips, tps, heads_a, heads_b, pivots, *refs),
+        name="attend_sliced",
+        out_shape=jax.ShapeDtypeStruct((rows, slices * 2 * DA), jnp.bfloat16),
+        in_specs=[any_space] * 2 + [pl.BlockSpec(memory_space=pltpu.SMEM), vmem, vmem],
+        out_specs=vmem,
+        scratch_shapes=[
+            pltpu.VMEM((chips * CORES, slices, rows, 4 * DA), jnp.bfloat16),
+            pltpu.VMEM((chips, slices, rows, 2 * DA), jnp.bfloat16),
+            pltpu.VMEM((chips, slices, 2, rows, 2 * DA), jnp.float32),
+            pltpu.VMEM((chips, slices, 4, rows, 1), jnp.float32),
+            pltpu.VMEM((chips, slices, 4, rows, 1), jnp.float32),
+            pltpu.VMEM((chips, slices, rows, 2 * DA), jnp.bfloat16),
+            pltpu.VMEM((slices, rows, 2 * DA), jnp.bfloat16),
+            dma((slices, 5)),
+            dma((slices,)),
+            dma((chips, slices)),
+            dma((slices,)),
+            dma((slices, chips - 1)),
+            dma((chips * CORES, slices)),
+            dma((chips, slices)),
+            dma((chips, slices)),
+            dma((slices,)),
+        ],
+        compiler_params=pltpu.CompilerParams(
+            collective_id=6, has_side_effects=True, vmem_limit_bytes=VMEM_BYTES
         ),
     )(queries, own, lambdas, gain_a, gain_b)
 
@@ -560,15 +921,17 @@
 
 def experts_kernel(
     chips, tps, capacity,
-    own_ref, meta_ref, gate_ref, up_ref, down_ref, out_ref,
+    own_ref, meta_ref, gate_ref, up_ref, down_ref, base_ref, gain_ref, out_ref,
     rows_all, meta_all, gate, up, down, rows_in, hidden, back, part, core_in, x_in, z_in,
+    z_other, sums,
     load_sem, weight_sem, row_sem, meta_send, meta_recv, up_sem, dn_sem, x_sem, side_sem,
     core_send, core_recv, xs_send, xs_recv, zs_send, zs_recv,
+    zo_send, zo_recv,
 ):
     chip, core, tp = place()
     experts = meta_ref.shape[0] // 2
     piece_rows, width = rows_all.shape[2], rows_all.shape[3]
-    rows = piece_rows * PIECES
+    rows = piece_rows * CUTS
     ff = gate.shape[1]
     members = CORES * tps
     side_sp = chip * CORES + 1 - core
@@ -609,7 +972,7 @@
     mine = blk(chip, core, tp)
     loads = [
         pltpu.make_async_copy(own_ref.at[piece], rows_all.at[mine, piece], load_sem.at[piece])
-        for piece in range(PIECES)
+        for piece in range(CUTS)
     ]
     weights = [
         pltpu.make_async_copy(src, dst, weight_sem.at[number])
@@ -620,7 +983,7 @@
     meta_all[mine] = meta_ref[...]
     meet(chips, tps)
 
-    for piece in range(PIECES):
+    for piece in range(CUTS):
         loads[piece].wait()
         for step in range(1, tps):
             go_x(chip, step, piece).start()
@@ -704,7 +1067,7 @@
                     (((0,), (0,)), ((), ())), preferred_element_type=jnp.float32,
                 ).astype(jnp.bfloat16)
                 part[group * members + member, :, :, cols] = spread.reshape(
-                    PIECES, piece_rows, wide
+                    CUTS, piece_rows, wide
                 )
 
     def add(target, index, source, source_index):
@@ -732,6 +1095,15 @@
                       zs_send.at[way, group, piece], zs_recv.at[way, group, piece],
                       (chip + 1 - 2 * way) * CORES + core, tp)
 
+    def other_z(way, step, piece):
+        group = chip + 1 - 2 * way
+        return remote(part.at[blk(group, core, (tp + step) % tps), piece],
+                      z_other.at[way, step - 1, piece], zo_send.at[way, step - 1, piece],
+                      zo_recv.at[way, step - 1, piece], group * CORES + core, tp)
+
+    def far(group):
+        return (group - chip >= 2) | (chip - group >= 2)
+
     def arrived(ref, sem):
         pltpu.make_async_copy(ref, ref, sem).wait()
 
@@ -741,16 +1113,25 @@
         for step in list(range(1, tps)) + [0]:
             tp_of = (tp + step) % tps
             arrived(core_in.at[group, tp_of], core_recv.at[group, tp_of])
-            for piece in range(PIECES):
+            for piece in range(CUTS):
                 add(part, (blk(group, core, tp_of), piece), core_in, (group, tp_of, piece))
                 if step > 0:
-                    part_x(group, step, piece).start()
+                    @pl.when(far(group))
+                    def _():
+                        part_x(group, step, piece).start()
+
+                    for way in range(2):
+                        @pl.when(group == chip + 1 - 2 * way)
+                        def _():
+                            other_z(way, step, piece).start()
 
     def settle(group):
-        for piece in range(PIECES):
-            for step in range(1, tps):
-                arrived(x_in.at[group, step - 1, piece], xs_recv.at[group, step - 1, piece])
-                add(part, (blk(group, core, tp), piece), x_in, (group, step - 1, piece))
+        for piece in range(CUTS):
+            @pl.when(far(group))
+            def _():
+                for step in range(1, tps):
+                    arrived(x_in.at[group, step - 1, piece], xs_recv.at[group, step - 1, piece])
+                    add(part, (blk(group, core, tp), piece), x_in, (group, step - 1, piece))
 
             @pl.when((chip == 0) & (group > 0))
             def _():
@@ -763,7 +1144,7 @@
     def wave(step, carry):
         @pl.when(step < chips)
         def _():
-            for piece in range(PIECES):
+            for piece in range(CUTS):
                 @pl.when(chip - step >= 0)
                 def _():
                     relay(chip - step, piece, True)
@@ -773,7 +1154,7 @@
                     relay(chip + step, piece, False)
 
         group = group_at(chip, chips, step - 1)
-        for piece in range(PIECES):
+        for piece in range(CUTS):
             for tp_step in range(1, tps):
                 tp_of = (tp + tp_step) % tps
                 wait_rows(blk(group, core, tp_of), piece)
@@ -787,7 +1168,7 @@
             for copy in weights:
                 copy.wait()
 
-        for piece in range(PIECES):
+        for piece in range(CUTS):
             for tp_of in range(tps):
                 wait_rows(blk(group, 1 - core, tp_of), piece)
         compute(group)
@@ -800,6 +1181,17 @@
         return carry
 
     lax.fori_loop(1, chips + 1, wave, 0)
+    for piece in range(CUTS):
+        for step in range(1, tps):
+            for way in range(2):
+                @pl.when(chip > 0 if way == 0 else chip < chips - 1)
+                def _():
+                    arrived(z_other.at[way, step - 1, piece], zo_recv.at[way, step - 1, piece])
+                    add(part, (blk(chip, core, (tp + step) % tps), piece), z_other,
+                        (way, step - 1, piece))
+
+            part_x(chip, step, piece).start()
+
     settle(group_at(chip, chips, chips - 1))
 
     def chain(number, carry):
@@ -812,7 +1204,7 @@
 
             @pl.when(passes)
             def _():
-                for piece in range(PIECES):
+                for piece in range(CUTS):
                     arrived(z_in.at[way, group, piece], zs_recv.at[way, group, piece])
                     add(part, (blk(group, core, tp), piece), z_in, (way, group, piece))
                     part_z(way, group, piece).start()
@@ -822,32 +1214,51 @@
     lax.fori_loop(1, chips, chain, 0)
 
     chunk = min(piece_rows, 16)
-    for piece in range(PIECES):
+
+    def each_chunk(body):
         @pl.loop(0, piece_rows // chunk)
         def _(number):
-            span = pl.ds(pl.multiple_of(number * chunk, chunk), chunk)
-            out_ref[piece, span, :] = part[mine, piece, span, :].astype(jnp.float32)
-
+            body(pl.ds(pl.multiple_of(number * chunk, chunk), chunk))
+
+    for piece in range(CUTS):
+        for step in range(1, tps):
+            arrived(x_in.at[chip, step - 1, piece], xs_recv.at[chip, step - 1, piece])
+
+        def begin(span):
+            start = part[mine, piece, span, :].astype(jnp.float32)
+            for step in range(1, tps):
+                start = start + x_in[chip, step - 1, piece, span, :].astype(jnp.float32)
+            sums[span, :] = start
+
+        each_chunk(begin)
         for way in range(2):
+            def more(span):
+                sums[span, :] = sums[span, :] + z_in[way, chip, piece, span, :].astype(jnp.float32)
+
             @pl.when(chip > 0 if way == 0 else chip < chips - 1)
             def _():
                 arrived(z_in.at[way, chip, piece], zs_recv.at[way, chip, piece])
-
-                @pl.loop(0, piece_rows // chunk)
-                def _(number):
-                    span = pl.ds(pl.multiple_of(number * chunk, chunk), chunk)
-                    out_ref[piece, span, :] = out_ref[piece, span, :] + z_in[
-                        way, chip, piece, span, :
-                    ].astype(jnp.float32)
+                each_chunk(more)
+
+        def close(span):
+            out_ref[piece, span, :] = (
+                base_ref[piece, span, :].astype(jnp.float32) + rms_norm(sums[span, :], gain_ref[...])
+            ).astype(out_ref.dtype)
+
+        each_chunk(close)
 
     for number, steps in enumerate(meta_steps):
         meta_copy(number, *steps).wait_send()
 
     def finish(group, carry):
-        for piece in range(PIECES):
+        for piece in range(CUTS):
             for step in range(1, tps):
                 go_x(group, step, piece).wait_send()
-                part_x(group, step, piece).wait_send()
+
+                @pl.when(far(group) | (group == chip))
+                def _():
+                    part_x(group, step, piece).wait_send()
+
             for tp_of in range(tps):
                 go_side(group, tp_of, piece).wait_send()
 
@@ -872,23 +1283,29 @@
         return carry
 
     lax.fori_loop(0, chips, finish, 0)
+    for piece in range(CUTS):
+        for step in range(1, tps):
+            for way in range(2):
+                @pl.when(chip < chips - 1 if way == 0 else chip > 0)
+                def _():
+                    other_z(way, step, piece).wait_send()
 
 
 def experts_bytes(rows, width, ff, chips, tps, capacity):
     blocks = chips * CORES * tps
     members = CORES * tps
-    buffers = blocks * 2 + chips * (2 * tps - 1 + 2) + 2
+    buffers = blocks * 2 + chips * (2 * tps - 1 + 2) + 2 * tps + 4
     return 2 * (
         rows * width * buffers + 3 * width * ff + members * capacity * (width + ff) + 2 * rows * width
     )
 
 
-def run_experts(normed, meta, gate, up, down, chips, tps, capacity):
+def run_experts(normed, meta, gate, up, down, base, gain, chips, tps, capacity):
     rows, width = normed.shape
     ff = gate.shape[1]
     blocks = chips * CORES * tps
     members = CORES * tps
-    piece_rows = rows // PIECES
+    piece_rows = rows // CUTS
     vmem = pl.BlockSpec(memory_space=pltpu.VMEM)
     any_space = pl.BlockSpec(memory_space=pl.ANY)
     dma = pltpu.SemaphoreType.DMA
@@ -896,11 +1313,11 @@
     return pl.pallas_call(
         lambda *refs: experts_kernel(chips, tps, capacity, *refs),
         name="run_experts",
-        out_shape=jax.ShapeDtypeStruct((PIECES, piece_rows, width), jnp.float32),
-        in_specs=[any_space, vmem, any_space, any_space, any_space],
+        out_shape=jax.ShapeDtypeStruct((CUTS, piece_rows, width), bf16),
+        in_specs=[any_space, vmem, any_space, any_space, any_space, vmem, vmem],
         out_specs=vmem,
         scratch_shapes=[
-            pltpu.VMEM((blocks, PIECES, piece_rows, width), bf16),
+            pltpu.VMEM((blocks, CUTS, piece_rows, width), bf16),
             pltpu.VMEM((blocks,) + meta.shape, meta.dtype),
             pltpu.VMEM(gate.shape, bf16),
             pltpu.VMEM(up.shape, bf16),
@@ -908,30 +1325,37 @@
             pltpu.VMEM((members * capacity, width), bf16),
             pltpu.VMEM((members * capacity, ff), bf16),
             pltpu.VMEM((members, capacity, rows), bf16),
-            pltpu.VMEM((blocks, PIECES, piece_rows, width), bf16),
-            pltpu.VMEM((chips, tps, PIECES, piece_rows, width), bf16),
-            pltpu.VMEM((chips, tps - 1, PIECES, piece_rows, width), bf16),
-            pltpu.VMEM((2, chips, PIECES, piece_rows, width), bf16),
-            dma((PIECES,)),
+            pltpu.VMEM((blocks, CUTS, piece_rows, width), bf16),
+            pltpu.VMEM((chips, tps, CUTS, piece_rows, width), bf16),
+            pltpu.VMEM((chips, tps - 1, CUTS, piece_rows, width), bf16),
+            pltpu.VMEM((2, chips, CUTS, piece_rows, width), bf16),
+            pltpu.VMEM((2, tps - 1, CUTS, piece_rows, width), bf16),
+            pltpu.VMEM((piece_rows, width), jnp.float32),
+            dma((CUTS,)),
             dma((3,)),
-            dma((blocks, PIECES)),
+            dma((blocks, CUTS)),
             dma((blocks - 1,)),
             dma((blocks,)),
-            dma((chips, PIECES)),
-            dma((chips, PIECES)),
-            dma((chips, tps - 1, PIECES)),
-            dma((chips, tps, PIECES)),
+            dma((chips, CUTS)),
+            dma((chips, CUTS)),
+            dma((chips, tps - 1, CUTS)),
+            dma((chips, tps, CUTS)),
             dma((chips, tps)),
             dma((chips, tps)),
-            dma((chips, tps - 1, PIECES)),
-            dma((chips, tps - 1, PIECES)),
-            dma((2, chips, PIECES)),
-            dma((2, chips, PIECES)),
+            dma((chips, tps - 1, CUTS)),
+            dma((chips, tps - 1, CUTS)),
+            dma((2, chips, CUTS)),
+            dma((2, chips, CUTS)),
+            dma((2, tps - 1, CUTS)),
+            dma((2, tps - 1, CUTS)),
         ],
         compiler_params=pltpu.CompilerParams(
             collective_id=5, has_side_effects=True, vmem_limit_bytes=VMEM_BYTES
         ),
-    )(normed.reshape(PIECES, piece_rows, width), meta, gate, up, down).reshape(rows, width)
+    )(
+        normed.reshape(CUTS, piece_rows, width), meta, gate, up, down,
+        base.reshape(CUTS, piece_rows, width), gain,
+    ).reshape(rows, width)
 
 
 def slot_table(routes, route_weights, experts):
@@ -991,24 +1415,34 @@
     heads_b = queries_b.shape[2] // DB
     head_slot = lax.axis_index("tp")
     seq_slot = lax.axis_index("sp")
-    lambda_a = lax.dynamic_slice_in_dim(lambdas, head_slot * heads_a, heads_a)
-    lambda_b = lax.dynamic_slice_in_dim(lambdas, HA + head_slot * heads_b, heads_b)
     experts, tps = lax.axis_size("sp"), lax.axis_size("tp")
     chips = experts // CORES
+    pivots = pivots_of(chips, heads_a + heads_b // 2)
     own = jnp.concatenate(
         [keys_a.reshape(length, -1), values_a, keys_b.reshape(length, -1), values_b], 1
     )
-    queries = jnp.concatenate([queries_a.reshape(length, -1), spread_pairs(queries_b, heads_b)], 1)
-    heads_out = attend_blocks(
-        queries,
-        own,
-        jnp.concatenate([lambda_a, lambda_b])[None],
-        head_gain_a[None],
-        head_gain_b[None],
-        chips,
-        heads_a,
-        heads_b,
-    )
+    if pivots is not None:
+        heads_out = attend_sliced(
+            jnp.concatenate([queries_a.reshape(length, -1), queries_b.reshape(length, -1)], 1),
+            own, lambdas[None], head_gain_a[None], head_gain_b[None], chips, tps, heads_a, heads_b,
+            pivots,
+        )
+    else:
+        lambda_a = lax.dynamic_slice_in_dim(lambdas, head_slot * heads_a, heads_a)
+        lambda_b = lax.dynamic_slice_in_dim(lambdas, HA + head_slot * heads_b, heads_b)
+        queries = jnp.concatenate(
+            [queries_a.reshape(length, -1), spread_pairs(queries_b, heads_b)], 1
+        )
+        heads_out = attend_blocks(
+            queries,
+            own,
+            jnp.concatenate([lambda_a, lambda_b])[None],
+            head_gain_a[None],
+            head_gain_b[None],
+            chips,
+            heads_a,
+            heads_b,
+        )
     cut = heads_a * 2 * DA
     mixed = (
         jnp.dot(heads_out[:, :cut], out_a, preferred_element_type=jnp.float32)
@@ -1023,15 +1457,14 @@
     width = residual.shape[1]
     slots = -(-capacity // 16) * 16
     if experts_bytes(sub_rows, width, expert_gate.shape[2], chips, tps, slots) < VMEM_BYTES * 9 // 10:
-        routed = run_experts(
+        return run_experts(
             normed, slot_table(routes, route_weights, experts), expert_gate[0], expert_up[0],
-            expert_down[0], chips, tps, slots,
-        )
-    else:
-        routed = spread_experts(
-            normed, routes, route_weights, seq_slot, experts, capacity, chips, tps,
-            (expert_gate[0], expert_up[0], expert_down[0]),
-        )
+            expert_down[0], after_mix, gain_post[None], chips, tps, slots,
+        )
+    routed = spread_experts(
+        normed, routes, route_weights, seq_slot, experts, capacity, chips, tps,
+        (expert_gate[0], expert_up[0], expert_down[0]),
+    )
     return (after_mix.astype(jnp.float32) + rms_norm(routed, gain_post)).astype(jnp.bfloat16)
 
 

time: 262 us -> 224 us (0.85)
  Pallas kernels: 243 us -> 208 us
  other arithmetic: 11 us -> 7.59 us
    pallas_call x1, Pallas kernels: 200 us -> 143 us  [run_experts(): pl.pallas_call(lambda *refs: experts_kernel(chips, tps, capacity, *refs),...]
    pallas_call x1, Pallas kernels: 28 us -> 49.7 us  [attend_sliced(): pl.pallas_call(lambda *refs: sliced_kernel(chips, tps, heads_a, heads_b,...]
    unnamed x32 -> x27, local copies, waits for them, and re-layouts: 1.26 us -> 4.11 us
where the time goes in v2:
time: 224 us; the launch traced here: 223 us
  Pallas kernels  208 us (93%)
  other arithmetic  7.59 us (3%)
  local copies, waits for them, and re-layouts  4.11 us (2%)
  matrix products  3.66 us (2%)
    pallas_call x1, Pallas kernels, run_experts(): pl.pallas_call(lambda *refs: experts_kernel(chips, tps, capacity, *refs),...  143 us
    pallas_call x1, Pallas kernels, attend_sliced(): pl.pallas_call(lambda *refs: sliced_kernel(chips, tps, heads_a, heads_b,...  49.7 us
    pallas_call x1, Pallas kernels, share_rows(): pl.pallas_call(lambda *refs: share_kernel(tps, *refs), name='share_rows',...  15 us

profile of v2, /device:TPU:0, one launch (start us, length us, event | category | flops | bytes accessed | tf_op | source)
XLA Modules:
  0.0 223.4 jit_solution(6879231900316915140)
XLA Ops:
  0.0 0.0 copy-start
  0.0 0.0 copy-start.5
  0.0 0.0 copy-start.6
  0.0 1.1 copy.25
  1.1 1.0 copy.26
  2.1 2.1 pad_maximum_fusion.refs_1_
  4.3 0.0 copy-done.5
  4.3 0.0 copy-done.6
  4.3 0.9 pad_maximum_fusion.1.refs_0_
  5.2 49.7 %attend_sliced.1 = bf16[256,1024]{1,0:T(8,128)(2,1)} custom-call(bf16[256,1024]{1,0:T(8,128)(2,1)} %pad_maximum_fusion.1.refs_0_, bf16[256,2048]{1,0:T(8,128)(2,1)} %pad_maximum_fusion.refs_1_, f32[1,12]{1,0:T(1,128)} %bitcast.39, f32[1,256]{1,0:T(1,128)} %bitcast.38, f32[1,128]{1,0:T(1,128)} %bitcast.40), custom_call_target="tpu_custom_call" | custom-call | tf_op jit(solution)/shard_map/attend_sliced/pallas_call | solution.py:778
  54.9 0.0 copy-done
  54.9 0.0 copy-start.2
  54.9 0.0 copy-start.3
  54.9 1.8 fusion.5
  56.7 0.0 copy-done.2
  56.8 0.0 copy-done.3
  56.8 1.7 fusion
  58.5 0.0 copy-start.4
  58.5 0.0 copy-start.7
  58.5 15.0 %share_rows.1 = f32[128,2048]{1,0:T(8,128)} custom-call(bf16[2,128,2048]{2,1,0:T(8,128)(2,1)} %bitcast.23), custom_call_target="tpu_custom_call" | custom-call | tf_op jit(solution)/shard_map/share_rows/pallas_call | solution.py:838
  73.5 0.0 copy-start.8
  73.5 0.0 copy-start.9
  73.6 0.0 copy-start.10
  73.6 1.4 multiply_reduce_fusion
  75.0 0.0 copy-done.4
  75.0 0.0 copy-done.7
  75.0 1.6 fusion.1
  76.6 0.0 copy-start.1
  76.6 0.0 copy-done.8
  76.6 1.0 fusion.3
  77.6 0.0 copy-done.9
  77.6 0.1 convolution_select_fusion
  77.7 0.0 copy-done.10
  77.8 0.6 pad_maximum_fusion.2.refs_1_
  78.4 0.0 copy-done.1
  78.4 143.2 %run_experts.1 = bf16[4,32,2048]{2,1,0:T(8,128)(2,1)} custom-call(bf16[4,32,2048]{2,1,0:T(8,128)(2,1)} %bitcast.28, f32[16,128]{1,0:T(8,128)} %pad_maximum_fusion.2.refs_1_, bf16[2048,1024]{1,0:T(8,128)(2,1)} %bitcast.24, bf16[2048,1024]{1,0:T(8,128)(2,1)} %bitcast.25, bf16[1024,2048]{1,0:T(8,128)(2,1)} %bitcast.26, bf16[4,32,2048]{2,1,0:T(8,128)(2,1)} %bitcast.22, ...), custom_call_target="tpu_custom_call" | custom-call | tf_op jit(solution)/shard_map/run_experts/pallas_call | solution.py:1313
  221.5 1.9 copy.28
  (6 shorter events, 0.1 us)
Async XLA Ops:
  0.0 54.9 %copy-start = (bf16[512,2048]{1,0:T(8,128)(2,1)S(1)}, bf16[512,2048]{1,0:T(8,128)(2,1)}, u32[]{:S(2)}) copy-start(bf16[512,2048]{1,0:T(8,128)(2,1)} %param.29) | copy-start | bytes 6291460
  0.0 4.3 %copy-start.5 = (bf16[256,2,256]{2,1,0:T(2,128)(2,1)S(1)}, bf16[256,2,256]{2,1,0:T(2,128)(2,1)}, u32[]{:S(2)}) copy-start(bf16[256,2,256]{2,1,0:T(2,128)(2,1)} %param.20) | copy-start | bytes 786436
  0.0 4.3 %copy-start.6 = (bf16[256,2,256]{2,1,0:T(2,128)(2,1)S(1)}, bf16[256,2,256]{2,1,0:T(2,128)(2,1)}, u32[]{:S(2)}) copy-start(bf16[256,2,256]{2,1,0:T(2,128)(2,1)} %param.23) | copy-start | bytes 786436
  54.9 1.8 copy-start.2
  54.9 1.8 copy-start.3
  58.5 16.5 %copy-start.4 = (bf16[128,2048]{1,0:T(8,128)(2,1)S(1)}, bf16[128,2048]{1,0:T(8,128)(2,1)}, u32[]{:S(2)}) copy-start(bf16[128,2048]{1,0:T(8,128)(2,1)} %param.31) | copy-start | bytes 1572868
  58.5 16.5 %copy-start.7 = (f32[2048]{0:T(1024)S(1)}, f32[2048]{0:T(1024)}, u32[]{:S(2)}) copy-start(f32[2048]{0:T(1024)} %param.32) | copy-start | bytes 24580
  73.5 3.1 %copy-start.8 = (f32[2048]{0:T(1024)S(1)}, f32[2048]{0:T(1024)}, u32[]{:S(2)}) copy-start(f32[2048]{0:T(1024)} %param.33) | copy-start | bytes 24580
  73.5 4.0 %copy-start.9 = (s32[128,4]{0,1:T(4,128)S(1)}, s32[128,4]{0,1:T(4,128)}, u32[]{:S(2)}) copy-start(s32[128,4]{0,1:T(4,128)} %param.35) | copy-start | bytes 6148
  73.6 4.2 %copy-start.10 = (f32[128,4]{0,1:T(4,128)S(1)}, f32[128,4]{0,1:T(4,128)}, u32[]{:S(2)}) copy-start(f32[128,4]{0,1:T(4,128)} %param.36) | copy-start | bytes 6148
  76.6 1.8 copy-start.1

commit v3 on v2

--- a/solution.py
+++ b/solution.py
@@ -538,7 +538,7 @@
         def _():
             send_side(chip, number).start()
 
-    for number in order:
+    for number in reversed(order):
         @pl.when(chip > pivots[number])
         def _():
             send_dn(number).start()
@@ -921,12 +921,14 @@
 
 def experts_kernel(
     chips, tps, capacity,
-    own_ref, meta_ref, gate_ref, up_ref, down_ref, base_ref, gain_ref, out_ref,
-    rows_all, meta_all, gate, up, down, rows_in, hidden, back, part, core_in, x_in, z_in,
-    z_other, sums,
+    heads_ref, out_a_ref, out_b_ref, residual_ref, gain_mix_ref, gain_pre_ref,
+    meta_ref, gate_ref, up_ref, down_ref, gain_ref, out_ref,
+    mixers, mix_out, mix_own, mix_in, base_ref, mix_send, mix_recv,
+    rows_all, meta_all, gate, up, down, rows_in, hidden, outs, back, part, core_in, x_in, z_in,
+    z_near, z_far, sums,
     load_sem, weight_sem, row_sem, meta_send, meta_recv, up_sem, dn_sem, x_sem, side_sem,
     core_send, core_recv, xs_send, xs_recv, zs_send, zs_recv,
-    zo_send, zo_recv,
+    zn_send, zn_recv, zf_recv,
 ):
     chip, core, tp = place()
     experts = meta_ref.shape[0] // 2
@@ -970,9 +972,10 @@
         pltpu.make_async_copy(ref, ref, row_sem.at[block, piece]).wait()
 
     mine = blk(chip, core, tp)
+    deep = out_a_ref.shape[0]
     loads = [
-        pltpu.make_async_copy(own_ref.at[piece], rows_all.at[mine, piece], load_sem.at[piece])
-        for piece in range(CUTS)
+        pltpu.make_async_copy(src, mixers.at[number], load_sem.at[number])
+        for number, src in enumerate((out_a_ref, out_b_ref))
     ]
     weights = [
         pltpu.make_async_copy(src, dst, weight_sem.at[number])
@@ -983,21 +986,6 @@
     meta_all[mine] = meta_ref[...]
     meet(chips, tps)
 
-    for piece in range(CUTS):
-        loads[piece].wait()
-        for step in range(1, tps):
-            go_x(chip, step, piece).start()
-
-        @pl.when(chip < chips - 1)
-        def _():
-            go_up(chip, piece).start()
-
-        @pl.when(chip > 0)
-        def _():
-            go_dn(chip, piece).start()
-
-        go_side(chip, tp, piece).start()
-
     def meta_copy(number, chip_step, core_step, tp_step):
         return remote(
             meta_ref, meta_all.at[mine], meta_send.at[number], meta_recv.at[mine],
@@ -1012,6 +1000,73 @@
     for number, steps in enumerate(meta_steps):
         meta_copy(number, *steps).start()
 
+    def project(tp_of, store):
+        wide = min(width, 512)
+        span = pl.ds(pl.multiple_of(tp_of * rows, rows), rows)
+
+        @pl.loop(0, width // wide)
+        def _(number):
+            cols = pl.ds(pl.multiple_of(number * wide, wide), wide)
+            made = sum(
+                jnp.dot(
+                    heads_ref[span, half * deep : (half + 1) * deep], mixers[half, :, cols],
+                    preferred_element_type=jnp.float32,
+                )
+                for half in range(2)
+            )
+            store(cols, made.astype(jnp.bfloat16).reshape(CUTS, piece_rows, wide))
+
+    def mix_copy(step, piece):
+        return remote(mix_out.at[step - 1, piece], mix_in.at[step - 1, piece],
+                      mix_send.at[step - 1, piece], mix_recv.at[step - 1, piece],
+                      chip * CORES + core, (tp + step) % tps)
+
+    for copy in loads:
+        copy.wait()
+    for step in range(1, tps):
+        def keep_other(cols, values):
+            mix_out[step - 1, :, :, cols] = values
+
+        project((tp + step) % tps, keep_other)
+        for piece in range(CUTS):
+            mix_copy(step, piece).start()
+
+    def keep_own(cols, values):
+        mix_own[:, :, cols] = values
+
+    project(tp, keep_own)
+    for piece in range(CUTS):
+        for step in range(1, tps):
+            ref = mix_in.at[step - 1, piece]
+            pltpu.make_async_copy(ref, ref, mix_recv.at[step - 1, piece]).wait()
+
+        @pl.loop(0, piece_rows // 16)
+        def _(number):
+            span = pl.ds(pl.multiple_of(number * 16, 16), 16)
+            mixed = mix_own[piece, span, :].astype(jnp.float32)
+            for step in range(1, tps):
+                mixed = mixed + mix_in[step - 1, piece, span, :].astype(jnp.float32)
+            after = (
+                residual_ref[piece, span, :].astype(jnp.float32) + rms_norm(mixed, gain_mix_ref[...])
+            ).astype(jnp.bfloat16)
+            base_ref[piece, span, :] = after
+            rows_all[mine, piece, span, :] = rms_norm(
+                after.astype(jnp.float32), gain_pre_ref[...]
+            ).astype(jnp.bfloat16)
+
+        for step in range(1, tps):
+            go_x(chip, step, piece).start()
+
+        @pl.when(chip < chips - 1)
+        def _():
+            go_up(chip, piece).start()
+
+        @pl.when(chip > 0)
+        def _():
+            go_dn(chip, piece).start()
+
+        go_side(chip, tp, piece).start()
+
     def relay(chip_of, piece, upward):
         wait_rows(blk(chip_of, core, tp), piece)
         for step in range(1, tps):
@@ -1026,24 +1081,31 @@
                 go_dn(chip_of, piece).start()
         go_side(chip_of, tp, piece).start()
 
-    def compute(group):
-        order = lax.broadcasted_iota(jnp.int32, (capacity, rows), 0).astype(jnp.float32)
+    def compute(group, between):
+        order = lax.broadcasted_iota(jnp.int32, (rows, rows), 0).astype(jnp.float32)
         expert = chip * CORES + core
+        between(0)
         for member in range(members):
             block = group * members + member
             slot = meta_all[block, pl.ds(expert, 1), :]
             share = meta_all[block, pl.ds(experts + expert, 1), :]
             hit = slot == order
-            picks = jnp.where(hit, 1.0, 0.0).astype(jnp.bfloat16)
-            back[member] = jnp.where(hit, share, 0.0).astype(jnp.bfloat16)
+            picks = jnp.where(hit[:capacity], 1.0, 0.0).astype(jnp.bfloat16)
+            back[member] = jnp.where(hit, share, 0.0).T.astype(jnp.bfloat16)
             values = rows_all[block].reshape(rows, width)
             rows_in[member * capacity : (member + 1) * capacity, :] = jnp.dot(
                 picks, values, preferred_element_type=jnp.float32
             ).astype(jnp.bfloat16)
-        cut = min(ff, 256)
+        cut = min(ff, 512)
+        wide = min(width, 512)
+        split = min(CUTS // 2, ff // cut)
 
         @pl.loop(0, ff // cut)
         def _(number):
+            @pl.when((number > 0) & (number < split))
+            def _():
+                between(number)
+
             cols = pl.ds(pl.multiple_of(number * cut, cut), cut)
             gate_pre = jnp.dot(rows_in[...], gate[:, cols], preferred_element_type=jnp.float32)
             up_pre = jnp.dot(rows_in[...], up[:, cols], preferred_element_type=jnp.float32)
@@ -1053,22 +1115,27 @@
                 glu_part * jax.nn.sigmoid(1.702 * glu_part) * (lin_part + 1.0)
             ).astype(jnp.bfloat16)
 
-        wide = min(width, 256)
-
         @pl.loop(0, width // wide)
         def _(number):
+            @pl.when(number + split < CUTS)
+            def _():
+                between(number + split)
+
             cols = pl.ds(pl.multiple_of(number * wide, wide), wide)
-            outs = jnp.dot(
+            outs[:, cols] = jnp.dot(
                 hidden[...], down[:, cols], preferred_element_type=jnp.float32
             ).astype(jnp.bfloat16)
-            for member in range(members):
-                spread = lax.dot_general(
-                    back[member], outs[member * capacity : (member + 1) * capacity],
-                    (((0,), (0,)), ((), ())), preferred_element_type=jnp.float32,
-                ).astype(jnp.bfloat16)
-                part[group * members + member, :, :, cols] = spread.reshape(
-                    CUTS, piece_rows, wide
-                )
+
+        for piece in range(split + width // wide, CUTS):
+            between(piece)
+
+        @pl.loop(0, members)
+        def _(member):
+            span = pl.ds(pl.multiple_of(member * capacity, 16), capacity)
+            spread = jnp.dot(
+                back[member, :, :capacity], outs[span, :], preferred_element_type=jnp.float32
+            ).astype(jnp.bfloat16)
+            part[group * members + member] = spread.reshape(CUTS, piece_rows, width)
 
     def add(target, index, source, source_index):
         chunk = min(piece_rows, 16)
@@ -1081,78 +1148,97 @@
                 + source[source_index + (span,)].astype(jnp.float32)
             ).astype(target.dtype)
 
-    def core_copy(group, tp_of):
-        return remote(part.at[blk(group, 1 - core, tp_of)], core_in.at[group, tp_of],
-                      core_send.at[group, tp_of], core_recv.at[group, tp_of], side_sp, tp)
+    def core_copy(group, tp_of, piece):
+        return remote(part.at[blk(group, 1 - core, tp_of), piece], core_in.at[group, tp_of, piece],
+                      core_send.at[group, tp_of, piece], core_recv.at[group, tp_of, piece],
+                      side_sp, tp)
 
     def part_x(group, step, piece):
         return remote(part.at[blk(group, core, (tp + step) % tps), piece],
                       x_in.at[group, step - 1, piece], xs_send.at[group, step - 1, piece],
                       xs_recv.at[group, step - 1, piece], chip * CORES + core, (tp + step) % tps)
 
-    def part_z(way, group, piece):
-        return remote(part.at[blk(group, core, tp), piece], z_in.at[way, group, piece],
-                      zs_send.at[way, group, piece], zs_recv.at[way, group, piece],
-                      (chip + 1 - 2 * way) * CORES + core, tp)
-
-    def other_z(way, step, piece):
+    def far_z(way, group, piece, last):
+        dst, recv, chip_to = (
+            (z_far.at[way, piece], zf_recv.at[way, piece], group) if last
+            else (z_in.at[way, group, piece], zs_recv.at[way, group, piece], chip + 1 - 2 * way)
+        )
+        return remote(part.at[blk(group, core, tp), piece], dst, zs_send.at[way, group, piece], recv,
+                      chip_to * CORES + core, tp)
+
+    def near_z(way, step, piece):
         group = chip + 1 - 2 * way
         return remote(part.at[blk(group, core, (tp + step) % tps), piece],
-                      z_other.at[way, step - 1, piece], zo_send.at[way, step - 1, piece],
-                      zo_recv.at[way, step - 1, piece], group * CORES + core, tp)
+                      z_near.at[way, step, piece], zn_send.at[way, step, piece],
+                      zn_recv.at[way, step, piece], group * CORES + core, tp)
+
+    def distance(way, group):
+        return group - chip if way == 0 else chip - group
 
     def far(group):
         return (group - chip >= 2) | (chip - group >= 2)
 
+    def go_far(way, group, piece):
+        @pl.when(distance(way, group) == 2)
+        def _():
+            far_z(way, group, piece, True).start()
+
+        @pl.when(distance(way, group) > 2)
+        def _():
+            far_z(way, group, piece, False).start()
+
     def arrived(ref, sem):
         pltpu.make_async_copy(ref, ref, sem).wait()
 
+    steps_x = list(range(1, tps)) + [0]
+
+    def hand_over(group):
+        for step in steps_x:
+            for piece in range(CUTS):
+                core_copy(group, (tp + step) % tps, piece).start()
+
     def cross(group):
-        for tp_of in range(tps):
-            core_copy(group, tp_of).start()
-        for step in list(range(1, tps)) + [0]:
+        for step in steps_x:
             tp_of = (tp + step) % tps
-            arrived(core_in.at[group, tp_of], core_recv.at[group, tp_of])
             for piece in range(CUTS):
+                arrived(core_in.at[group, tp_of, piece], core_recv.at[group, tp_of, piece])
                 add(part, (blk(group, core, tp_of), piece), core_in, (group, tp_of, piece))
                 if step > 0:
                     @pl.when(far(group))
                     def _():
                         part_x(group, step, piece).start()
 
-                    for way in range(2):
-                        @pl.when(group == chip + 1 - 2 * way)
-                        def _():
-                            other_z(way, step, piece).start()
+                for way in range(2):
+                    @pl.when(distance(way, group) == 1)
+                    def _():
+                        near_z(way, step, piece).start()
 
     def settle(group):
-        for piece in range(CUTS):
-            @pl.when(far(group))
-            def _():
+        @pl.when(far(group))
+        def _():
+            for piece in range(CUTS):
                 for step in range(1, tps):
                     arrived(x_in.at[group, step - 1, piece], xs_recv.at[group, step - 1, piece])
                     add(part, (blk(group, core, tp), piece), x_in, (group, step - 1, piece))
 
-            @pl.when((chip == 0) & (group > 0))
-            def _():
-                part_z(0, group, piece).start()
-
-            @pl.when((chip == chips - 1) & (group < chips - 1))
-            def _():
-                part_z(1, group, piece).start()
+                @pl.when((chip == 0) & (group > 0))
+                def _():
+                    go_far(0, group, piece)
+
+                @pl.when((chip == chips - 1) & (group < chips - 1))
+                def _():
+                    go_far(1, group, piece)
+
+    def relays(step, piece):
+        @pl.when((step < chips) & (chip - step >= 0))
+        def _():
+            relay(chip - step, piece, True)
+
+        @pl.when((step < chips) & (chip + step < chips))
+        def _():
+            relay(chip + step, piece, False)
 
     def wave(step, carry):
-        @pl.when(step < chips)
-        def _():
-            for piece in range(CUTS):
-                @pl.when(chip - step >= 0)
-                def _():
-                    relay(chip - step, piece, True)
-
-                @pl.when(chip + step < chips)
-                def _():
-                    relay(chip + step, piece, False)
-
         group = group_at(chip, chips, step - 1)
         for piece in range(CUTS):
             for tp_step in range(1, tps):
@@ -1171,24 +1257,35 @@
         for piece in range(CUTS):
             for tp_of in range(tps):
                 wait_rows(blk(group, 1 - core, tp_of), piece)
-        compute(group)
-        cross(group)
-
-        @pl.when(step > 1)
-        def _():
-            settle(group_at(chip, chips, step - 2))
+        compute(group, lambda piece: relays(step + 1, piece))
+        hand_over(group)
+        before = group_at(chip, chips, step - 2)
+
+        @pl.when((step > 1) & jnp.logical_not(far(before)))
+        def _():
+            cross(before)
+
+        @pl.when(far(group) | (step == chips))
+        def _():
+            cross(group)
+
+        @pl.when((step > 1) & far(before))
+        def _():
+            settle(before)
 
         return carry
 
+    for piece in range(CUTS):
+        relays(1, piece)
     lax.fori_loop(1, chips + 1, wave, 0)
     for piece in range(CUTS):
         for step in range(1, tps):
             for way in range(2):
                 @pl.when(chip > 0 if way == 0 else chip < chips - 1)
                 def _():
-                    arrived(z_other.at[way, step - 1, piece], zo_recv.at[way, step - 1, piece])
-                    add(part, (blk(chip, core, (tp + step) % tps), piece), z_other,
-                        (way, step - 1, piece))
+                    arrived(z_near.at[way, step, piece], zn_recv.at[way, step, piece])
+                    add(part, (blk(chip, core, (tp + step) % tps), piece), z_near,
+                        (way, step, piece))
 
             part_x(chip, step, piece).start()
 
@@ -1197,17 +1294,14 @@
     def chain(number, carry):
         for way in range(2):
             group = number if way == 0 else chips - 1 - number
-            if way == 0:
-                passes = (chip > 0) & (chip < group)
-            else:
-                passes = (chip < chips - 1) & (chip > group)
-
-            @pl.when(passes)
+            starts = chip == 0 if way == 0 else chip == chips - 1
+
+            @pl.when((distance(way, group) >= 2) & jnp.logical_not(starts))
             def _():
                 for piece in range(CUTS):
                     arrived(z_in.at[way, group, piece], zs_recv.at[way, group, piece])
                     add(part, (blk(group, core, tp), piece), z_in, (way, group, piece))
-                    part_z(way, group, piece).start()
+                    go_far(way, group, piece)
 
         return carry
 
@@ -1233,12 +1327,22 @@
         each_chunk(begin)
         for way in range(2):
             def more(span):
-                sums[span, :] = sums[span, :] + z_in[way, chip, piece, span, :].astype(jnp.float32)
-
-            @pl.when(chip > 0 if way == 0 else chip < chips - 1)
-            def _():
-                arrived(z_in.at[way, chip, piece], zs_recv.at[way, chip, piece])
+                sums[span, :] = sums[span, :] + z_near[way, 0, piece, span, :].astype(jnp.float32)
+
+            def most(span):
+                sums[span, :] = sums[span, :] + z_far[way, piece, span, :].astype(jnp.float32)
+
+            behind = chip if way == 0 else chips - 1 - chip
+
+            @pl.when(behind > 0)
+            def _():
+                arrived(z_near.at[way, 0, piece], zn_recv.at[way, 0, piece])
                 each_chunk(more)
+
+            @pl.when(behind > 1)
+            def _():
+                arrived(z_far.at[way, piece], zf_recv.at[way, piece])
+                each_chunk(most)
 
         def close(span):
             out_ref[piece, span, :] = (
@@ -1249,6 +1353,9 @@
 
     for number, steps in enumerate(meta_steps):
         meta_copy(number, *steps).wait_send()
+    for piece in range(CUTS):
+        for step in range(1, tps):
+            mix_copy(step, piece).wait_send()
 
     def finish(group, carry):
         for piece in range(CUTS):
@@ -1270,38 +1377,38 @@
             def _():
                 go_dn(group, piece).wait_send()
 
-            @pl.when(group > chip)
-            def _():
-                part_z(0, group, piece).wait_send()
-
-            @pl.when(group < chip)
-            def _():
-                part_z(1, group, piece).wait_send()
-
-        for tp_of in range(tps):
-            core_copy(group, tp_of).wait_send()
+            for way in range(2):
+                @pl.when(distance(way, group) >= 2)
+                def _():
+                    far_z(way, group, piece, True).wait_send()
+
+            for tp_of in range(tps):
+                core_copy(group, tp_of, piece).wait_send()
+
         return carry
 
     lax.fori_loop(0, chips, finish, 0)
     for piece in range(CUTS):
-        for step in range(1, tps):
+        for step in range(tps):
             for way in range(2):
                 @pl.when(chip < chips - 1 if way == 0 else chip > 0)
                 def _():
-                    other_z(way, step, piece).wait_send()
-
-
-def experts_bytes(rows, width, ff, chips, tps, capacity):
+                    near_z(way, step, piece).wait_send()
+
+
+def experts_bytes(rows, width, ff, deep, chips, tps, capacity):
     blocks = chips * CORES * tps
     members = CORES * tps
-    buffers = blocks * 2 + chips * (2 * tps - 1 + 2) + 2 * tps + 4
+    buffers = blocks * 2 + chips * (2 * tps - 1 + 2) + 2 * tps + 8
     return 2 * (
-        rows * width * buffers + 3 * width * ff + members * capacity * (width + ff) + 2 * rows * width
+        rows * width * buffers + 3 * width * ff + members * capacity * (2 * width + ff) + 4 * rows * width
+        + 2 * deep * (width + rows * tps) + (2 * tps + 1) * rows * width
     )
 
 
-def run_experts(normed, meta, gate, up, down, base, gain, chips, tps, capacity):
-    rows, width = normed.shape
+def run_experts(heads_out, mixers, residual, gains, meta, weights, chips, tps, capacity):
+    rows, width = residual.shape
+    gate, up, down = weights
     ff = gate.shape[1]
     blocks = chips * CORES * tps
     members = CORES * tps
@@ -1314,9 +1421,16 @@
         lambda *refs: experts_kernel(chips, tps, capacity, *refs),
         name="run_experts",
         out_shape=jax.ShapeDtypeStruct((CUTS, piece_rows, width), bf16),
-        in_specs=[any_space, vmem, any_space, any_space, any_space, vmem, vmem],
+        in_specs=[vmem, any_space, any_space] + [vmem] * 4 + [any_space] * 3 + [vmem],
         out_specs=vmem,
         scratch_shapes=[
+            pltpu.VMEM((2,) + mixers[0].shape, bf16),
+            pltpu.VMEM((tps - 1, CUTS, piece_rows, width), bf16),
+            pltpu.VMEM((CUTS, piece_rows, width), bf16),
+            pltpu.VMEM((tps - 1, CUTS, piece_rows, width), bf16),
+            pltpu.VMEM((CUTS, piece_rows, width), bf16),
+            dma((tps - 1, CUTS)),
+            dma((tps - 1, CUTS)),
             pltpu.VMEM((blocks, CUTS, piece_rows, width), bf16),
             pltpu.VMEM((blocks,) + meta.shape, meta.dtype),
             pltpu.VMEM(gate.shape, bf16),
@@ -1324,14 +1438,16 @@
             pltpu.VMEM(down.shape, bf16),
             pltpu.VMEM((members * capacity, width), bf16),
             pltpu.VMEM((members * capacity, ff), bf16),
-            pltpu.VMEM((members, capacity, rows), bf16),
+            pltpu.VMEM((members * capacity, width), bf16),
+            pltpu.VMEM((members, rows, rows), bf16),
             pltpu.VMEM((blocks, CUTS, piece_rows, width), bf16),
             pltpu.VMEM((chips, tps, CUTS, piece_rows, width), bf16),
             pltpu.VMEM((chips, tps - 1, CUTS, piece_rows, width), bf16),
             pltpu.VMEM((2, chips, CUTS, piece_rows, width), bf16),
-            pltpu.VMEM((2, tps - 1, CUTS, piece_rows, width), bf16),
+            pltpu.VMEM((2, tps, CUTS, piece_rows, width), bf16),
+            pltpu.VMEM((2, CUTS, piece_rows, width), bf16),
             pltpu.VMEM((piece_rows, width), jnp.float32),
-            dma((CUTS,)),
+            dma((2,)),
             dma((3,)),
             dma((blocks, CUTS)),
             dma((blocks - 1,)),
@@ -1340,21 +1456,22 @@
             dma((chips, CUTS)),
             dma((chips, tps - 1, CUTS)),
             dma((chips, tps, CUTS)),
-            dma((chips, tps)),
-            dma((chips, tps)),
+            dma((chips, tps, CUTS)),
+            dma((chips, tps, CUTS)),
             dma((chips, tps - 1, CUTS)),
             dma((chips, tps - 1, CUTS)),
             dma((2, chips, CUTS)),
             dma((2, chips, CUTS)),
-            dma((2, tps - 1, CUTS)),
-            dma((2, tps - 1, CUTS)),
+            dma((2, tps, CUTS)),
+            dma((2, tps, CUTS)),
+            dma((2, CUTS)),
         ],
         compiler_params=pltpu.CompilerParams(
             collective_id=5, has_side_effects=True, vmem_limit_bytes=VMEM_BYTES
         ),
     )(
-        normed.reshape(CUTS, piece_rows, width), meta, gate, up, down,
-        base.reshape(CUTS, piece_rows, width), gain,
+        heads_out, *mixers, residual.reshape(CUTS, piece_rows, width), gains[0], gains[1], meta, gate, up,
+        down, gains[2],
     ).reshape(rows, width)
 
 
@@ -1443,7 +1560,19 @@
             heads_a,
             heads_b,
         )
+    sub_rows = residual.shape[0]
+    top_count = routes.shape[1]
+    capacity = min(sub_rows, (5 * sub_rows * top_count + 4 * experts - 1) // (4 * experts))
+    width = residual.shape[1]
+    slots = -(-capacity // 16) * 16
+    weights = (expert_gate[0], expert_up[0], expert_down[0])
     cut = heads_a * 2 * DA
+    need = experts_bytes(sub_rows, width, weights[0].shape[1], cut, chips, tps, slots)
+    if out_a.shape == out_b.shape and need < VMEM_BYTES:
+        return run_experts(
+            heads_out, (out_a, out_b), residual, (gain_mix[None], gain_pre[None], gain_post[None]),
+            slot_table(routes, route_weights, experts), weights, chips, tps, slots,
+        )
     mixed = (
         jnp.dot(heads_out[:, :cut], out_a, preferred_element_type=jnp.float32)
         + jnp.dot(heads_out[:, cut:], out_b, preferred_element_type=jnp.float32)
@@ -1451,19 +1580,9 @@
     mixed_rows = share_rows(mixed.reshape(tps, length // tps, -1), tps)
     after_mix = (residual.astype(jnp.float32) + rms_norm(mixed_rows, gain_mix)).astype(jnp.bfloat16)
     normed = rms_norm(after_mix.astype(jnp.float32), gain_pre).astype(jnp.bfloat16)
-    sub_rows = residual.shape[0]
-    top_count = routes.shape[1]
-    capacity = min(sub_rows, (5 * sub_rows * top_count + 4 * experts - 1) // (4 * experts))
-    width = residual.shape[1]
-    slots = -(-capacity // 16) * 16
-    if experts_bytes(sub_rows, width, expert_gate.shape[2], chips, tps, slots) < VMEM_BYTES * 9 // 10:
-        return run_experts(
-            normed, slot_table(routes, route_weights, experts), expert_gate[0], expert_up[0],
-            expert_down[0], after_mix, gain_post[None], chips, tps, slots,
-        )
     routed = spread_experts(
         normed, routes, route_weights, seq_slot, experts, capacity, chips, tps,
-        (expert_gate[0], expert_up[0], expert_down[0]),
+        weights,
     )
     return (after_mix.astype(jnp.float32) + rms_norm(routed, gain_post)).astype(jnp.bfloat16)
 

time: 224 us -> 196 us (0.88)
  the two profiles are of different devices: /device:TPU:0 before, /device:TPU:25 now
where the time goes in v3:
time: 196 us; the launch traced here: 195 us
  Pallas kernels  187 us (95%)
  local copies, waits for them, and re-layouts  3.98 us (2%)
  other arithmetic  3.61 us (2%)
    pallas_call x1, Pallas kernels, run_experts(): pl.pallas_call(lambda *refs: experts_kernel(chips, tps, capacity, *refs),...  129 us
    pallas_call x1, Pallas kernels, attend_sliced(): pl.pallas_call(lambda *refs: sliced_kernel(chips, tps, heads_a, heads_b,...  58.2 us
    unnamed x13, local copies, waits for them, and re-layouts  3.98 us

profile of v3, /device:TPU:25, one launch (start us, length us, event | category | flops | bytes accessed | tf_op | source)
XLA Modules:
  0.0 195.3 jit_solution(1854249395902783554)
XLA Ops:
  0.0 0.0 copy-start
  0.0 0.0 copy-start.1
  0.0 1.0 copy.25
  1.0 1.0 copy.26
  2.0 2.1 %pad_maximum_fusion.refs_1_ = bf16[256,2048]{1,0:T(8,128)(2,1)} fusion(bf16[256,512]{1,0:T(8,128)(2,1)} %param.25, bf16[256,512]{1,0:T(8,128)(2,1)S(1)} %bitcast.27, bf16[256,512]{1,0:T(8,128)(2,1)} %param.22, bf16[256,512]{1,0:T(8,128)(2,1)S(1)} %bitcast.26), kind=kLoop, calls=%fused_computation.1 | loop fusion | flops 4194304 | bytes 2097152 | tf_op jit(solution)/shard_map/concatenate | solution.py:1538
  4.2 0.0 copy-done
  4.2 0.0 copy-start.2
  4.2 0.0 copy-start.3
  4.2 0.0 copy-done.1
  4.3 0.9 pad_maximum_fusion.1.refs_0_
  5.1 58.2 %attend_sliced.1.refs_0_ = bf16[256,1024]{1,0:T(8,128)(2,1)} custom-call(bf16[256,1024]{1,0:T(8,128)(2,1)} %pad_maximum_fusion.1.refs_0_, bf16[256,2048]{1,0:T(8,128)(2,1)} %pad_maximum_fusion.refs_1_, f32[1,12]{1,0:T(1,128)} %bitcast.37, f32[1,256]{1,0:T(1,128)} %bitcast.36, f32[1,128]{1,0:T(1,128)} %bitcast.38), custom_call_target="tpu_custom_call" | custom-call | tf_op jit(solution)/shard_map/attend_sliced/pallas_call | solution.py:778
  63.3 0.0 copy-done.2
  63.4 0.1 convolution_select_fusion
  63.5 0.0 copy-done.3
  63.5 0.6 pad_maximum_fusion.2.refs_6_
  64.1 129.3 %run_experts.1 = bf16[4,32,2048]{2,1,0:T(8,128)(2,1)} custom-call(bf16[256,1024]{1,0:T(8,128)(2,1)} %attend_sliced.1.refs_0_, bf16[512,2048]{1,0:T(8,128)(2,1)} %refs_1_.1, bf16[512,2048]{1,0:T(8,128)(2,1)} %refs_2_.1, bf16[4,32,2048]{2,1,0:T(8,128)(2,1)} %bitcast.28, f32[1,2048]{1,0:T(1,128)} %bitcast.33, f32[1,2048]{1,0:T(1,128)} %bitcast.34, ...), custom_call_target="tpu_custom_call" | custom-call | tf_op jit(solution)/shard_map/run_experts/pallas_call | solution.py:1420
  193.4 1.9 copy.28
  (4 shorter events, 0.1 us)
Async XLA Ops:
  0.0 4.2 %copy-start = (bf16[256,2,256]{2,1,0:T(2,128)(2,1)S(1)}, bf16[256,2,256]{2,1,0:T(2,128)(2,1)}, u32[]{:S(2)}) copy-start(bf16[256,2,256]{2,1,0:T(2,128)(2,1)} %param.20) | copy-start | bytes 786436
  0.0 4.2 %copy-start.1 = (bf16[256,2,256]{2,1,0:T(2,128)(2,1)S(1)}, bf16[256,2,256]{2,1,0:T(2,128)(2,1)}, u32[]{:S(2)}) copy-start(bf16[256,2,256]{2,1,0:T(2,128)(2,1)} %param.23) | copy-start | bytes 786436
  4.2 59.2 %copy-start.2 = (s32[128,4]{0,1:T(4,128)S(1)}, s32[128,4]{0,1:T(4,128)}, u32[]{:S(2)}) copy-start(s32[128,4]{0,1:T(4,128)} %param.35) | copy-start | bytes 6148
  4.2 59.3 %copy-start.3 = (f32[128,4]{0,1:T(4,128)S(1)}, f32[128,4]{0,1:T(4,128)}, u32[]{:S(2)}) copy-start(f32[128,4]{0,1:T(4,128)} %param.36) | copy-start | bytes 6148

commit v4 on v3

--- a/solution.py
+++ b/solution.py
@@ -17,7 +17,8 @@
 MESH = pl.DeviceIdType.MESH
 CORES = 2
 PIECES = 2
-CUTS = 4
+CUTS = 2
+EARLY = ()
 LOG2E = 1.4426950408889634
 VMEM_BYTES = 60 * 1024 * 1024
 
@@ -451,7 +452,7 @@
 
 def sliced_kernel(
     chips, tps, heads_a, heads_b, pivots,
-    q_ref, own_ref, lambda_ref, gain_a_ref, gain_b_ref, out_ref,
+    q_ref, k_ref, va_ref, vb_ref, lambda_ref, gain_a_ref, gain_b_ref, out_ref,
     kvs, qs, accum, top, total, o_out, o_all,
     load_sem, q_send, q_recv, dn_send, up_send, kv_recv, side_send, o_send, o_recv,
 ):
@@ -469,19 +470,17 @@
     loads = []
     for number in range(slices):
         if number < heads_a:
-            head, stride, q_at, k_at = number, heads_a * DA, 0, 0
+            head, stride, base, v_ref = number, heads_a * DA, 0, va_ref
         else:
-            head, stride = number - heads_a, heads_b * DB
-            q_at, k_at = 2 * heads_a * DA, 4 * heads_a * DA
-        v_at = k_at + 2 * stride + head * 2 * DA
+            head, stride, base, v_ref = number - heads_a, heads_b * DB, 2 * heads_a * DA, vb_ref
         moves = []
         for pair in range(2):
-            at = pair * stride + head * DA
+            cols = pl.ds(base + pair * stride + head * DA, DA)
             spot = pl.ds(pair * DA, DA)
-            moves.append((q_ref.at[:, pl.ds(q_at + at, DA)], qs.at[chip, number, :, spot]))
-            moves.append((own_ref.at[:, pl.ds(k_at + at, DA)], kvs.at[me, number, :, spot]))
+            moves.append((q_ref.at[:, cols], qs.at[chip, number, :, spot]))
+            moves.append((k_ref.at[:, cols], kvs.at[me, number, :, spot]))
         moves.append(
-            (own_ref.at[:, pl.ds(v_at, 2 * DA)], kvs.at[me, number, :, pl.ds(key_width, 2 * DA)])
+            (v_ref.at[:, pl.ds(head * 2 * DA, 2 * DA)], kvs.at[me, number, :, pl.ds(key_width, 2 * DA)])
         )
         loads.append([
             pltpu.make_async_copy(src, dst, load_sem.at[number, place_in])
@@ -538,7 +537,7 @@
         def _():
             send_side(chip, number).start()
 
-    for number in reversed(order):
+    for number in order:
         @pl.when(chip > pivots[number])
         def _():
             send_dn(number).start()
@@ -615,25 +614,22 @@
         lax.fori_loop(0, heads_a, run_a, 0)
         lax.fori_loop(heads_a, slices, run_b, 0)
 
-    def pair_up(query, kv_chip, first):
-        def body(number, flash):
-            @pl.when(relevant(query, number))
-            def _():
-                @pl.when(first)
-                def _():
-                    top[query, number] = jnp.full(top.shape[2:], -1e30, jnp.float32)
-                    total[query, number] = jnp.zeros(total.shape[2:], jnp.float32)
-                    accum[query, number] = jnp.zeros(accum.shape[2:], jnp.float32)
-
-                @pl.when(query == kv_chip)
-                def _():
-                    flash(query, kv_chip, number, True)
-
-                @pl.when(query != kv_chip)
-                def _():
-                    flash(query, kv_chip, number, False)
-
-        over(body)
+    def pair_up(query, kv_chip, first, number, flash):
+        @pl.when(relevant(query, number))
+        def _():
+            @pl.when(first)
+            def _():
+                top[query, number] = jnp.full(top.shape[2:], -1e30, jnp.float32)
+                total[query, number] = jnp.zeros(total.shape[2:], jnp.float32)
+                accum[query, number] = jnp.zeros(accum.shape[2:], jnp.float32)
+
+            @pl.when(query == kv_chip)
+            def _():
+                flash(query, kv_chip, number, True)
+
+            @pl.when(query != kv_chip)
+            def _():
+                flash(query, kv_chip, number, False)
 
     def mix(query, number, slots, spans, lam, gain_ref):
         mixture = (
@@ -642,40 +638,37 @@
         )
         return rms_norm(mixture, gain_ref[...]).astype(jnp.bfloat16)
 
-    def finish(query):
-        def body(number, flash):
-            @pl.when(relevant(query, number))
-            def _():
-                if flash is flash_a:
-                    lam = lambda_ref[0, tp * heads_a + number]
-                    made = [mix(query, number, (0, 1), slice(0, 2 * DA), lam, gain_a_ref)]
-                else:
-                    made = []
-                    for head in range(2):
-                        lam = lambda_ref[
-                            0, tps * heads_a + tp * heads_b + (number - heads_a) * 2 + head
-                        ]
-                        made.append(
-                            mix(query, number, (head, 2 + head),
-                                slice(head * 2 * DB, (head + 1) * 2 * DB), lam, gain_b_ref)
-                        )
-                wide = 2 * DA // len(made)
-                for place_in, values in enumerate(made):
-                    span = slice(place_in * wide, (place_in + 1) * wide)
-
-                    @pl.when(query == chip)
-                    def _():
-                        o_all[number, :, span] = values
-
-                    @pl.when(query != chip)
-                    def _():
-                        o_out[query, number, :, span] = values
+    def finish(query, number, flash):
+        @pl.when(relevant(query, number))
+        def _():
+            if flash is flash_a:
+                lam = lambda_ref[0, tp * heads_a + number]
+                made = [mix(query, number, (0, 1), slice(0, 2 * DA), lam, gain_a_ref)]
+            else:
+                made = []
+                for head in range(2):
+                    lam = lambda_ref[
+                        0, tps * heads_a + tp * heads_b + (number - heads_a) * 2 + head
+                    ]
+                    made.append(
+                        mix(query, number, (head, 2 + head),
+                            slice(head * 2 * DB, (head + 1) * 2 * DB), lam, gain_b_ref)
+                    )
+            wide = 2 * DA // len(made)
+            for place_in, values in enumerate(made):
+                span = slice(place_in * wide, (place_in + 1) * wide)
+
+                @pl.when(query == chip)
+                def _():
+                    o_all[number, :, span] = values
 
                 @pl.when(query != chip)
                 def _():
-                    send_out(query, number).start()
-
-        over(body)
+                    o_out[query, number, :, span] = values
+
+            @pl.when(query != chip)
+            def _():
+                send_out(query, number).start()
 
     above = chips - 1 - chip
 
@@ -720,23 +713,26 @@
 
             return carry
 
-        lax.fori_loop(0, slices, wait_q, 0)
-        lax.fori_loop(0, slices, wait_kv, 0)
-        lax.fori_loop(0, slices, wait_side, 0)
-
-        def queries(query, carry):
-            pair_up(query, kv_chip, kv_chip == chip)
-
-            @pl.when(
-                ((query == chip) & (number_of == jnp.where(chip > 0, above + chip, 0)))
-                | (is_above & (query == source))
-            )
-            def _():
-                finish(query)
-
-            return carry
-
-        lax.fori_loop(low, high + 1, queries, 0)
+        def body(number, flash):
+            wait_q(number, 0)
+            wait_kv(number, 0)
+            wait_side(number, 0)
+
+            def queries(query, carry):
+                pair_up(query, kv_chip, kv_chip == chip, number, flash)
+
+                @pl.when(
+                    ((query == chip) & (number_of == jnp.where(chip > 0, above + chip, 0)))
+                    | (is_above & (query == source))
+                )
+                def _():
+                    finish(query, number, flash)
+
+                return carry
+
+            lax.fori_loop(low, high + 1, queries, 0)
+
+        over(body)
         return carry
 
     lax.fori_loop(0, 1 + above + chips - 1, event, 0)
@@ -769,8 +765,8 @@
                 send_out(chip_of, number).wait_send()
 
 
-def attend_sliced(queries, own, lambdas, gain_a, gain_b, chips, tps, heads_a, heads_b, pivots):
-    rows = own.shape[0]
+def attend_sliced(queries, keys, values, lambdas, gain_a, gain_b, chips, tps, heads_a, heads_b, pivots):
+    rows = keys.shape[0]
     slices = len(pivots)
     vmem = pl.BlockSpec(memory_space=pltpu.VMEM)
     any_space = pl.BlockSpec(memory_space=pl.ANY)
@@ -779,7 +775,7 @@
         lambda *refs: sliced_kernel(chips, tps, heads_a, heads_b, pivots, *refs),
         name="attend_sliced",
         out_shape=jax.ShapeDtypeStruct((rows, slices * 2 * DA), jnp.bfloat16),
-        in_specs=[any_space] * 2 + [pl.BlockSpec(memory_space=pltpu.SMEM), vmem, vmem],
+        in_specs=[any_space] * 4 + [pl.BlockSpec(memory_space=pltpu.SMEM), vmem, vmem],
         out_specs=vmem,
         scratch_shapes=[
             pltpu.VMEM((chips * CORES, slices, rows, 4 * DA), jnp.bfloat16),
@@ -802,7 +798,7 @@
         compiler_params=pltpu.CompilerParams(
             collective_id=6, has_side_effects=True, vmem_limit_bytes=VMEM_BYTES
         ),
-    )(queries, own, lambdas, gain_a, gain_b)
+    )(queries, keys, *values, lambdas, gain_a, gain_b)
 
 
 def share_kernel(tps, part_ref, out_ref, arrived, send_sem, recv_sem):
@@ -951,13 +947,26 @@
         ref = rows_all.at[block, piece]
         return remote(ref, ref, send, row_sem.at[block, piece], sp_to, tp_to)
 
-    def go_up(chip_of, piece):
-        return rows_copy(blk(chip_of, core, tp), piece, up_sem.at[chip_of, piece],
-                         (chip + 1) * CORES + core, tp)
-
-    def go_dn(chip_of, piece):
-        return rows_copy(blk(chip_of, core, tp), piece, dn_sem.at[chip_of, piece],
-                         (chip - 1) * CORES + core, tp)
+    def go_up(chip_of, step, piece):
+        return rows_copy(blk(chip_of, core, (tp + step) % tps), piece,
+                         up_sem.at[chip_of, step, piece], (chip + 1) * CORES + core, tp)
+
+    def go_dn(chip_of, step, piece):
+        return rows_copy(blk(chip_of, core, (tp + step) % tps), piece,
+                         dn_sem.at[chip_of, step, piece], (chip - 1) * CORES + core, tp)
+
+    def go_on(chip_of, step, piece, upward, downward):
+        if upward:
+            @pl.when(chip < chips - 1)
+            def _():
+                go_up(chip_of, step, piece).start()
+
+        if downward:
+            @pl.when(chip > 0)
+            def _():
+                go_dn(chip_of, step, piece).start()
+
+        go_side(chip_of, (tp + step) % tps, piece).start()
 
     def go_x(chip_of, step, piece):
         return rows_copy(blk(chip_of, core, tp), piece, x_sem.at[chip_of, step - 1, piece],
@@ -1057,29 +1066,20 @@
         for step in range(1, tps):
             go_x(chip, step, piece).start()
 
-        @pl.when(chip < chips - 1)
-        def _():
-            go_up(chip, piece).start()
-
-        @pl.when(chip > 0)
-        def _():
-            go_dn(chip, piece).start()
-
-        go_side(chip, tp, piece).start()
+        go_on(chip, 0, piece, True, True)
+
+    for piece in EARLY:
+        for step in range(1, tps):
+            wait_rows(blk(chip, core, (tp + step) % tps), piece)
+            go_on(chip, step, piece, True, True)
 
     def relay(chip_of, piece, upward):
-        wait_rows(blk(chip_of, core, tp), piece)
-        for step in range(1, tps):
-            go_x(chip_of, step, piece).start()
-        if upward:
-            @pl.when(chip < chips - 1)
-            def _():
-                go_up(chip_of, piece).start()
-        else:
-            @pl.when(chip > 0)
-            def _():
-                go_dn(chip_of, piece).start()
-        go_side(chip_of, tp, piece).start()
+        for step in range(tps if piece in EARLY else 1):
+            wait_rows(blk(chip_of, core, (tp + step) % tps), piece)
+            if piece not in EARLY:
+                for tp_step in range(1, tps):
+                    go_x(chip_of, tp_step, piece).start()
+            go_on(chip_of, step, piece, upward, not upward)
 
     def compute(group, between):
         order = lax.broadcasted_iota(jnp.int32, (rows, rows), 0).astype(jnp.float32)
@@ -1102,9 +1102,10 @@
 
         @pl.loop(0, ff // cut)
         def _(number):
-            @pl.when((number > 0) & (number < split))
-            def _():
-                between(number)
+            for piece in range(1, split):
+                @pl.when(number == piece)
+                def _():
+                    between(piece)
 
             cols = pl.ds(pl.multiple_of(number * cut, cut), cut)
             gate_pre = jnp.dot(rows_in[...], gate[:, cols], preferred_element_type=jnp.float32)
@@ -1117,9 +1118,10 @@
 
         @pl.loop(0, width // wide)
         def _(number):
-            @pl.when(number + split < CUTS)
-            def _():
-                between(number + split)
+            for piece in range(split, min(CUTS, split + width // wide)):
+                @pl.when(number + split == piece)
+                def _():
+                    between(piece)
 
             cols = pl.ds(pl.multiple_of(number * wide, wide), wide)
             outs[:, cols] = jnp.dot(
@@ -1241,10 +1243,11 @@
     def wave(step, carry):
         group = group_at(chip, chips, step - 1)
         for piece in range(CUTS):
-            for tp_step in range(1, tps):
-                tp_of = (tp + tp_step) % tps
-                wait_rows(blk(group, core, tp_of), piece)
-                go_side(group, tp_of, piece).start()
+            if piece not in EARLY:
+                for tp_step in range(1, tps):
+                    tp_of = (tp + tp_step) % tps
+                    wait_rows(blk(group, core, tp_of), piece)
+                    go_side(group, tp_of, piece).start()
 
         @pl.when(step == 1)
         def _():
@@ -1259,15 +1262,8 @@
                 wait_rows(blk(group, 1 - core, tp_of), piece)
         compute(group, lambda piece: relays(step + 1, piece))
         hand_over(group)
+        cross(group)
         before = group_at(chip, chips, step - 2)
-
-        @pl.when((step > 1) & jnp.logical_not(far(before)))
-        def _():
-            cross(before)
-
-        @pl.when(far(group) | (step == chips))
-        def _():
-            cross(group)
 
         @pl.when((step > 1) & far(before))
         def _():
@@ -1360,7 +1356,9 @@
     def finish(group, carry):
         for piece in range(CUTS):
             for step in range(1, tps):
-                go_x(group, step, piece).wait_send()
+                @pl.when((group == chip) | (piece not in EARLY))
+                def _():
+                    go_x(group, step, piece).wait_send()
 
                 @pl.when(far(group) | (group == chip))
                 def _():
@@ -1369,13 +1367,14 @@
             for tp_of in range(tps):
                 go_side(group, tp_of, piece).wait_send()
 
-            @pl.when((group <= chip) & (chip < chips - 1))
-            def _():
-                go_up(group, piece).wait_send()
-
-            @pl.when((group >= chip) & (chip > 0))
-            def _():
-                go_dn(group, piece).wait_send()
+            for step in range(tps if piece in EARLY else 1):
+                @pl.when((group <= chip) & (chip < chips - 1))
+                def _():
+                    go_up(group, step, piece).wait_send()
+
+                @pl.when((group >= chip) & (chip > 0))
+                def _():
+                    go_dn(group, step, piece).wait_send()
 
             for way in range(2):
                 @pl.when(distance(way, group) >= 2)
@@ -1452,8 +1451,8 @@
             dma((blocks, CUTS)),
             dma((blocks - 1,)),
             dma((blocks,)),
-            dma((chips, CUTS)),
-            dma((chips, CUTS)),
+            dma((chips, tps, CUTS)),
+            dma((chips, tps, CUTS)),
             dma((chips, tps - 1, CUTS)),
             dma((chips, tps, CUTS)),
             dma((chips, tps, CUTS)),
@@ -1535,18 +1534,19 @@
     experts, tps = lax.axis_size("sp"), lax.axis_size("tp")
     chips = experts // CORES
     pivots = pivots_of(chips, heads_a + heads_b // 2)
-    own = jnp.concatenate(
-        [keys_a.reshape(length, -1), values_a, keys_b.reshape(length, -1), values_b], 1
-    )
     if pivots is not None:
         heads_out = attend_sliced(
             jnp.concatenate([queries_a.reshape(length, -1), queries_b.reshape(length, -1)], 1),
-            own, lambdas[None], head_gain_a[None], head_gain_b[None], chips, tps, heads_a, heads_b,
-            pivots,
+            jnp.concatenate([keys_a.reshape(length, -1), keys_b.reshape(length, -1)], 1),
+            (values_a, values_b), lambdas[None], head_gain_a[None], head_gain_b[None], chips, tps,
+            heads_a, heads_b, pivots,
         )
     else:
         lambda_a = lax.dynamic_slice_in_dim(lambdas, head_slot * heads_a, heads_a)
         lambda_b = lax.dynamic_slice_in_dim(lambdas, HA + head_slot * heads_b, heads_b)
+        own = jnp.concatenate(
+            [keys_a.reshape(length, -1), values_a, keys_b.reshape(length, -1), values_b], 1
+        )
         queries = jnp.concatenate(
             [queries_a.reshape(length, -1), spread_pairs(queries_b, heads_b)], 1
         )

time: 196 us -> 183 us (0.934)
  the two profiles are of different devices: /device:TPU:25 before, /device:TPU:0 now
where the time goes in v4:
time: 183 us
  Pallas kernels  175 us (96%)
  local copies, waits for them, and re-layouts  5.85 us (3%)
    pallas_call x1, Pallas kernels, run_experts(): pl.pallas_call(lambda *refs: experts_kernel(chips, tps, capacity, *refs),...  125 us
    pallas_call x1, Pallas kernels, attend_sliced(): pl.pallas_call(lambda *refs: sliced_kernel(chips, tps, heads_a, heads_b,...  49.5 us
    unnamed x9, local copies, waits for them, and re-layouts  5.85 us

profile of v4, /device:TPU:0, one launch (start us, length us, event | category | flops | bytes accessed | tf_op | source)
XLA Modules:
  0.0 182.7 jit_solution(11255527864419058967)
XLA Ops:
  0.0 0.0 copy-start
  0.0 0.0 copy-start.1
  0.0 1.0 copy.23
  1.0 1.0 copy.24
  2.0 1.0 copy.25
  3.0 1.0 copy.26
  4.0 1.1 pad_maximum_fusion
  5.1 49.5 %attend_sliced.1.refs_0_ = bf16[256,1024]{1,0:T(8,128)(2,1)} custom-call(bf16[256,1024]{1,0:T(8,128)(2,1)} %get-tuple-element.5.refs_0_, bf16[256,1024]{1,0:T(8,128)(2,1)} %get-tuple-element.6.refs_1_, bf16[256,512]{1,0:T(8,128)(2,1)} %refs_2_.2, bf16[256,512]{1,0:T(8,128)(2,1)} %refs_3_.1, f32[1,12]{1,0:T(1,128)} %bitcast.37, f32[1,256]{1,0:T(1,128)} %bitcast.36, ...), custom_call_target="tpu_custom_call" | custom-call | tf_op jit(solution)/shard_map/attend_sliced/pallas_call | solution.py:774
  54.6 0.0 copy-done
  54.6 0.1 convolution_select_fusion
  54.8 0.0 copy-done.1
  54.8 0.6 pad_maximum_fusion.2.refs_6_
  55.4 125.5 %run_experts.1 = bf16[2,64,2048]{2,1,0:T(8,128)(2,1)} custom-call(bf16[256,1024]{1,0:T(8,128)(2,1)} %attend_sliced.1.refs_0_, bf16[512,2048]{1,0:T(8,128)(2,1)} %refs_1_.1, bf16[512,2048]{1,0:T(8,128)(2,1)} %refs_2_.3, bf16[2,64,2048]{2,1,0:T(8,128)(2,1)} %bitcast.28, f32[1,2048]{1,0:T(1,128)} %bitcast.33, f32[1,2048]{1,0:T(1,128)} %bitcast.34, ...), custom_call_target="tpu_custom_call" | custom-call | tf_op jit(solution)/shard_map/run_experts/pallas_call | solution.py:1419
  180.8 1.9 %copy.28 = bf16[128,2048]{1,0:T(8,128)(2,1)} copy(bf16[128,2048]{1,0:T(8,128)(2,1)} %bitcast.23) | data formatting | bytes 1048576
  (2 shorter events, 0.0 us)
Async XLA Ops:
  0.0 54.6 %copy-start = (s32[128,4]{0,1:T(4,128)S(1)}, s32[128,4]{0,1:T(4,128)}, u32[]{:S(2)}) copy-start(s32[128,4]{0,1:T(4,128)} %param.35) | copy-start | bytes 6148
  0.0 54.8 %copy-start.1 = (f32[128,4]{0,1:T(4,128)S(1)}, f32[128,4]{0,1:T(4,128)}, u32[]{:S(2)}) copy-start(f32[128,4]{0,1:T(4,128)} %param.36) | copy-start | bytes 6148

commit v5 on v4

--- a/solution.py
+++ b/solution.py
@@ -990,7 +990,7 @@
         pltpu.make_async_copy(src, dst, weight_sem.at[number])
         for number, (src, dst) in enumerate(((gate_ref, gate), (up_ref, up), (down_ref, down)))
     ]
-    for copy in loads + weights:
+    for copy in loads:
         copy.start()
     meta_all[mine] = meta_ref[...]
     meet(chips, tps)
@@ -1032,6 +1032,8 @@
 
     for copy in loads:
         copy.wait()
+    for copy in weights:
+        copy.start()
     for step in range(1, tps):
         def keep_other(cols, values):
             mix_out[step - 1, :, :, cols] = values

time: 183 us -> 183 us (level)
  no operation moved by 1% of the time
where the time goes in v5:
time: 183 us; the launch traced here: 181 us
  Pallas kernels  174 us (95%)
  local copies, waits for them, and re-layouts  5.85 us (3%)
    pallas_call x1, Pallas kernels, run_experts(): pl.pallas_call(lambda *refs: experts_kernel(chips, tps, capacity, *refs),...  124 us
    pallas_call x1, Pallas kernels, attend_sliced(): pl.pallas_call(lambda *refs: sliced_kernel(chips, tps, heads_a, heads_b,...  49.5 us
    unnamed x9, local copies, waits for them, and re-layouts  5.85 us

profile of v5, /device:TPU:0, one launch (start us, length us, event | category | flops | bytes accessed | tf_op | source)
XLA Modules:
  0.0 181.3 jit_solution(2182444095521085470)
XLA Ops:
  0.0 0.0 copy-start
  0.0 0.0 copy-start.1
  0.0 1.0 copy.23
  1.0 1.0 copy.24
  2.0 1.0 copy.25
  3.0 1.0 copy.26
  4.0 1.1 pad_maximum_fusion
  5.1 49.5 %attend_sliced.1.refs_0_ = bf16[256,1024]{1,0:T(8,128)(2,1)} custom-call(bf16[256,1024]{1,0:T(8,128)(2,1)} %get-tuple-element.5.refs_0_, bf16[256,1024]{1,0:T(8,128)(2,1)} %get-tuple-element.6.refs_1_, bf16[256,512]{1,0:T(8,128)(2,1)} %refs_2_.2, bf16[256,512]{1,0:T(8,128)(2,1)} %refs_3_.1, f32[1,12]{1,0:T(1,128)} %bitcast.37, f32[1,256]{1,0:T(1,128)} %bitcast.36, ...), custom_call_target="tpu_custom_call" | custom-call | tf_op jit(solution)/shard_map/attend_sliced/pallas_call | solution.py:774
  54.6 0.0 copy-done
  54.6 0.1 convolution_select_fusion
  54.8 0.0 copy-done.1
  54.8 0.6 pad_maximum_fusion.2.refs_6_
  55.4 124.1 %run_experts.1 = bf16[2,64,2048]{2,1,0:T(8,128)(2,1)} custom-call(bf16[256,1024]{1,0:T(8,128)(2,1)} %attend_sliced.1.refs_0_, bf16[512,2048]{1,0:T(8,128)(2,1)} %refs_1_.1, bf16[512,2048]{1,0:T(8,128)(2,1)} %refs_2_.3, bf16[2,64,2048]{2,1,0:T(8,128)(2,1)} %bitcast.28, f32[1,2048]{1,0:T(1,128)} %bitcast.33, f32[1,2048]{1,0:T(1,128)} %bitcast.34, ...), custom_call_target="tpu_custom_call" | custom-call | tf_op jit(solution)/shard_map/run_experts/pallas_call | solution.py:1421
  179.4 1.9 %copy.28 = bf16[128,2048]{1,0:T(8,128)(2,1)} copy(bf16[128,2048]{1,0:T(8,128)(2,1)} %bitcast.23) | data formatting | bytes 1048576
  (2 shorter events, 0.0 us)
Async XLA Ops:
  0.0 54.6 %copy-start = (s32[128,4]{0,1:T(4,128)S(1)}, s32[128,4]{0,1:T(4,128)}, u32[]{:S(2)}) copy-start(s32[128,4]{0,1:T(4,128)} %param.35) | copy-start | bytes 6148
  0.0 54.8 %copy-start.1 = (f32[128,4]{0,1:T(4,128)S(1)}, f32[128,4]{0,1:T(4,128)}, u32[]{:S(2)}) copy-start(f32[128,4]{0,1:T(4,128)} %param.36) | copy-start | bytes 6148
